TPU v7x, 32 devices: a whole 2x2x4 slice. The times are simulated.
32 devices in a mesh: sp: 4 (over z), fs: 4 (over y, x), tp: 2 (over core).
Axes of the slice: x: 2, y: 2, z: 4, core: 2. Of those that a mesh axis runs over, the one named last changes fastest.
Arguments:
- state_head_inputs: bfloat16 [4, 512, 1024], P('fs', 'sp', 'tp'), may hold values from -6 to 6
- state_write_vectors: bfloat16 [4, 512, 256], P('fs', 'sp', 'tp'), may hold values from -3 to 3
- state_read_vectors: bfloat16 [4, 512, 256], P('fs', 'sp', 'tp'), may hold values from -3 to 3
- state_output_gate: bfloat16 [4, 512, 1024], P('fs', 'sp', 'tp'), may hold values from -6 to 6
- presoftplus_steps: float32 [4, 16, 512], P('fs', 'tp', 'sp'), may hold values from -6 to 6
- extra_decay_log: float32 [4, 16, 512], P('fs', 'tp', 'sp'), may hold values from -2.1 to 0, as said below
- lane_shrinkage_powers: float32 [16], P('tp')
- bypass_coefficient_vector: float32 [16], P('tp'), may hold values from 0.5 to 4
- feeder_smoothing_stencil: bfloat16 [4, 1024], P(None, 'tp'), may hold values from -3 to 3
- stored_smoothing_stencil: bfloat16 [4, 256], P(None, 'tp'), may hold values from -3 to 3
- lookup_smoothing_stencil: bfloat16 [4, 256], P(None, 'tp'), may hold values from -3 to 3
- bundled_rescaling_vector: float32 [1024], P('tp'), may hold values from 0.1 to 1.9
- queries: bfloat16 [4, 512, 1024], P('fs', 'sp', 'tp'), may hold values from -8 to 8
- attention_keys: bfloat16 [4, 512, 256], P('fs', 'sp', 'tp'), may hold values from -8 to 8
- attention_values: bfloat16 [4, 512, 256], P('fs', 'sp', 'tp'), may hold values from -6 to 6
- forget_gate_cumsum: float32 [4, 512, 16], P('fs', 'sp', 'tp'), as said below
- state_out_weight: bfloat16 [1024, 2048], P('tp', 'fs'), may hold values from -0.1875 to 0.1875
- attention_out_weight: bfloat16 [1024, 2048], P('tp', 'fs'), may hold values from -0.75 to 0.75
Outputs:
- layer_output: bfloat16 [4, 512, 2048], P('fs', ('sp', 'tp'))
Inputs may be any that keep to these rules, and one draw needn't show every extreme that they name: `extra_decay_log`: nonpositive. `forget_gate_cumsum`: never rises along the positions of a sequence.
All inputs are finite; a program needn't handle non-finite values.
Results may differ from a plain program's by a relative error of at most 0.019.
Values may be sent and summed in bfloat16 or wider, within the bound.
A program may use at most 64 MiB of HBM per device.

v0:
```python
import functools
import math

import jax
import jax.numpy as jnp
from jax import lax
from jax.experimental import pallas as pl
from jax.experimental.pallas import tpu as pltpu
from jax.sharding import PartitionSpec as P

HEAD_DIM = 64
STATE = 128


EPSILON = 1e-06
NEGATIVE = -1e30


def passed_along(shard, axis, by):
    devices = lax.axis_size(axis)
    pairs = [(i, i + by) for i in range(devices) if 0 <= i + by < devices]
    return lax.ppermute(shard, axis, pairs)


def entering(shard, axis, join, neutral):
    place = lax.axis_index(axis)
    gathered = jax.tree.map(
        lambda a, kind: lax.all_gather(a.astype(kind), axis), shard, (jnp.bfloat16, jnp.bfloat16)
    )
    state = jax.tree.map(lambda a, e: jnp.zeros_like(a) + jnp.asarray(e, a.dtype), shard, neutral)

    def one(hop, state):
        return join(
            state,
            jax.tree.map(
                lambda a, own: lax.dynamic_index_in_dim(a, hop, 0, False).astype(own.dtype),
                gathered,
                shard,
            ),
        )

    return lax.fori_loop(0, place, one, state)


def causal_filter(feeder_quantities, before, taps):
    length = feeder_quantities.shape[0]
    padded = jnp.concatenate([before, feeder_quantities], axis=0).astype(jnp.float32)
    summed = jnp.zeros(feeder_quantities.shape, jnp.float32)
    for offset in range(taps.shape[0]):
        summed = summed + taps[offset].astype(jnp.float32) * padded[offset : offset + length]
    return jax.nn.silu(summed).astype(jnp.bfloat16)


def compose(earlier, later):
    return (earlier[0] * later[0], earlier[1] * later[0][..., None, None] + later[1])


def shards(
    state_head_inputs,
    state_write_vectors,
    state_read_vectors,
    state_output_gate,
    presoftplus_steps,
    extra_decay_log,
    lane_shrinkage_powers,
    bypass_coefficient_vector,
    feeder_smoothing_stencil,
    stored_smoothing_stencil,
    lookup_smoothing_stencil,
    bundled_rescaling_vector,
    queries,
    attention_keys,
    attention_values,
    forget_gate_cumsum,
    state_out_weight,
    attention_out_weight,
):
    shard_rows = state_head_inputs.shape[1]
    input_rows = state_head_inputs[0]
    write_rows = state_write_vectors[0]
    read_rows = state_read_vectors[0]
    tap_rows = feeder_smoothing_stencil.shape[0] - 1
    value_width = input_rows.shape[1]
    vector_width = write_rows.shape[1]
    tail_rows = jnp.concatenate(
        [input_rows[-tap_rows:], write_rows[-tap_rows:], read_rows[-tap_rows:]], axis=1
    )
    before = passed_along(tail_rows, "sp", 1)
    conv_values = causal_filter(input_rows, before[:, :value_width], feeder_smoothing_stencil)
    conv_write = causal_filter(
        write_rows, before[:, value_width : value_width + vector_width], stored_smoothing_stencil
    )
    conv_read = causal_filter(
        read_rows, before[:, value_width + vector_width :], lookup_smoothing_stencil
    )
    stride_duration = jax.nn.softplus(presoftplus_steps[0])
    shrinkage_natural_power = (
        stride_duration * (-jnp.exp(lane_shrinkage_powers))[:, None] + extra_decay_log[0]
    )
    lane_tally = stride_duration.shape[0]
    groups = vector_width // STATE
    per_group = lane_tally // groups
    cumulative = jnp.cumsum(shrinkage_natural_power, axis=1)
    input_heads = conv_values.reshape(shard_rows, groups, per_group, HEAD_DIM)
    write_groups = conv_write.reshape(shard_rows, groups, STATE)
    read_groups = conv_read.reshape(shard_rows, groups, STATE)
    inner_products = jnp.einsum(
        "tgn,sgn->gts", read_groups, write_groups, preferred_element_type=jnp.float32
    )
    positions = jnp.arange(shard_rows)
    causal = positions[:, None] >= positions[None, :]
    log_gap = jnp.where(causal[None], cumulative[:, :, None] - cumulative[:, None, :], -jnp.inf)
    weights = jnp.exp(log_gap) * stride_duration[:, None, :]
    mix_weights = (
        inner_products[:, None] * weights.reshape(groups, per_group, shard_rows, shard_rows)
    ).astype(jnp.bfloat16)
    local_part = jnp.einsum(
        "ghts,sghp->tghp", mix_weights, input_heads, preferred_element_type=jnp.float32
    )
    end_scale = (jnp.exp(cumulative[:, -1:] - cumulative) * stride_duration).T.reshape(
        shard_rows, groups, per_group
    )
    weighted = (input_heads.astype(jnp.float32) * end_scale[..., None]).astype(jnp.bfloat16)
    block_state = jnp.einsum(
        "sghp,sgn->ghpn", weighted, write_groups, preferred_element_type=jnp.float32
    )
    total_decay = jnp.exp(cumulative[:, -1]).reshape(groups, per_group)
    identity = (jnp.ones_like(total_decay), jnp.zeros_like(block_state))
    carried = entering((total_decay, block_state), "sp", compose, identity)[1]
    carried_part = jnp.einsum(
        "tgn,ghpn->tghp",
        read_groups,
        carried.astype(jnp.bfloat16),
        preferred_element_type=jnp.float32,
    )
    carried_part = (
        carried_part * jnp.exp(cumulative).T.reshape(shard_rows, groups, per_group)[..., None]
    )
    mixer_sum = (
        local_part
        + carried_part
        + bypass_coefficient_vector.reshape(groups, per_group)[None, :, :, None]
        * input_heads.astype(jnp.float32)
    )
    gated_rows = mixer_sum.reshape(shard_rows, groups, per_group * HEAD_DIM) * jax.nn.silu(
        state_output_gate[0].astype(jnp.float32)
    ).reshape(shard_rows, groups, -1)
    stretch_coefficient = lax.rsqrt(
        jnp.mean(gated_rows * gated_rows, axis=-1, keepdims=True) + EPSILON
    )
    state_result = (
        (gated_rows * stretch_coefficient * bundled_rescaling_vector.reshape(groups, -1))
        .reshape(shard_rows, -1)
        .astype(jnp.bfloat16)
    )
    attend_heads = forget_gate_cumsum.shape[2]
    key_group_count = attention_keys.shape[2] // HEAD_DIM
    repeat_factor = attend_heads // key_group_count
    query_head_count = queries[0].reshape(shard_rows, key_group_count, repeat_factor, HEAD_DIM)
    first_query = lax.axis_index("sp") * shard_rows
    query_index = first_query + jnp.arange(shard_rows)
    last_query = first_query + shard_rows - 1
    query_gates = forget_gate_cumsum[0].T
    all_gates = lax.all_gather(forget_gate_cumsum[0], "sp", axis=0, tiled=True)
    attention_score_scale = HEAD_DIM ** (-0.5)
    starting = (
        jnp.full((attend_heads, shard_rows), NEGATIVE, jnp.float32),
        jnp.zeros((attend_heads, shard_rows), jnp.float32),
        jnp.zeros((attend_heads, shard_rows, HEAD_DIM), jnp.float32),
    )
    key_rows = lax.all_gather(attention_keys[0], "sp", axis=0, tiled=True)
    value_rows = lax.all_gather(attention_values[0], "sp", axis=0, tiled=True)
    span = key_rows.shape[0]
    sub_block = math.gcd(span, 512)

    def advance(sub_index, running):
        first_key = sub_index * sub_block

        def attend(running):
            running_max, running_sum, weighted_sum = running
            key_tile = lax.dynamic_slice_in_dim(
                key_rows, sub_index * sub_block, sub_block, 0
            ).reshape(sub_block, key_group_count, HEAD_DIM)
            value_tile = lax.dynamic_slice_in_dim(
                value_rows, sub_index * sub_block, sub_block, 0
            ).reshape(sub_block, key_group_count, HEAD_DIM)
            key_gates = lax.dynamic_slice_in_dim(all_gates, first_key, sub_block, 0)
            attention_scores = jnp.einsum(
                "ezxp,czp->zxec", query_head_count, key_tile, preferred_element_type=jnp.float32
            )
            attention_scores = (
                attention_scores.reshape(attend_heads, shard_rows, sub_block)
                * attention_score_scale
            )
            attention_scores = attention_scores + query_gates[:, :, None] - key_gates.T[:, None, :]
            visible = (first_key + jnp.arange(sub_block))[None, :] <= query_index[:, None]
            attention_scores = jnp.where(visible[None], attention_scores, NEGATIVE)
            new_max = jnp.maximum(running_max, jnp.max(attention_scores, axis=-1))
            shrink = jnp.exp(running_max - new_max)
            attention_probs = jnp.where(
                visible[None], jnp.exp(attention_scores - new_max[..., None]), 0.0
            )
            running_sum = running_sum * shrink + jnp.sum(attention_probs, axis=-1)
            weighted_value_sum = jnp.einsum(
                "fljx,xfc->fljc",
                attention_probs.astype(jnp.bfloat16).reshape(
                    key_group_count, repeat_factor, shard_rows, sub_block
                ),
                value_tile,
                preferred_element_type=jnp.float32,
            )
            weighted_sum = weighted_sum * shrink[..., None] + weighted_value_sum.reshape(
                attend_heads, shard_rows, HEAD_DIM
            )
            return (new_max, running_sum, weighted_sum)

        return lax.cond(first_key <= last_query, attend, lambda kept: kept, running)

    _, running_sum, weighted_sum = lax.fori_loop(0, span // sub_block, advance, starting)
    attend_out = (
        (weighted_sum / running_sum[..., None])
        .transpose(1, 0, 2)
        .reshape(shard_rows, -1)
        .astype(jnp.bfloat16)
    )
    state_columns, attend_columns = (
        lax.all_gather(state_out_weight, "fs", axis=1, tiled=True),
        lax.all_gather(attention_out_weight, "fs", axis=1, tiled=True),
    )
    summed = lax.psum_scatter(
        (
            jnp.dot(state_result, state_columns, preferred_element_type=jnp.float32)
            + jnp.dot(attend_out, attend_columns, preferred_element_type=jnp.float32)
        ).astype(jnp.bfloat16),
        "tp",
        scatter_dimension=0,
        tiled=True,
    )
    return summed[None]


MESH = pl.DeviceIdType.MESH
LANES = 128
BF16, F32 = jnp.bfloat16, jnp.float32


def mixer_kernel(
    sp,
    fs,
    x_ref,
    w_ref,
    r_ref,
    gate_ref,
    step_ref,
    extra_ref,
    shrink_ref,
    bypass_ref,
    tapx_ref,
    tapw_ref,
    tapr_ref,
    gain_ref,
    q_ref,
    k_ref,
    v_ref,
    forget_ref,
    wst_far,
    wat_far,
    out_ref,
    wst_ref,
    wat_ref,
    load_sem,
    pad_ref,
    tails,
    conv,
    end_wide,
    kall,
    vall,
    gall,
    qs,
    own_state,
    state_in,
    state_out,
    mix,
    acts,
    pieces,
    scales,
    acc,
    acc_state,
    half_out,
    half_in,
    sums,
    landed,
    tail_send,
    tail_recv,
    kv_send,
    kv_recv,
    st_send,
    st_recv,
    act_send,
    act_recv,
    piece_send,
    piece_recv,
    half_send,
    half_recv,
    sum_send,
    sum_recv,
):
    me = lax.axis_index("sp")
    f = lax.axis_index("fs")
    t = lax.axis_index("tp")
    rows, width = x_ref.shape[1], x_ref.shape[2]
    heads = step_ref.shape[1]
    kv_heads = k_ref.shape[2] // HEAD_DIM
    repeat = heads // kv_heads
    pairs = heads // 2
    taps = tapx_ref.shape[0]
    cols = wst_far.shape[1]
    half = rows // 2

    loads = [
        pltpu.make_async_copy(far, near, load_sem.at[i])
        for i, (far, near) in enumerate(((wst_far, wst_ref), (wat_far, wat_ref)))
    ]
    for load in loads:
        load.start()

    barrier = pltpu.get_barrier_semaphore()
    for d in range(1, sp):
        pl.semaphore_signal(
            barrier, inc=1, device_id={"sp": lax.rem(me + d, sp)}, device_id_type=MESH
        )
    for d in range(1, fs):
        pl.semaphore_signal(
            barrier, inc=1, device_id={"fs": lax.rem(f + d, fs)}, device_id_type=MESH
        )
    pl.semaphore_signal(barrier, inc=1, device_id={"tp": 1 - t}, device_id_type=MESH)

    def remote(src, dst, send, recv, where):
        return pltpu.make_async_remote_copy(
            src_ref=src,
            dst_ref=dst,
            send_sem=send,
            recv_sem=recv,
            device_id=where,
            device_id_type=MESH,
        )

    lane = lax.broadcasted_iota(jnp.int32, (1, LANES), 1)
    low = lane < HEAD_DIM
    row_id = lax.broadcasted_iota(jnp.int32, (rows, rows), 0)
    col_id = lax.broadcasted_iota(jnp.int32, (rows, rows), 1)

    def expand(columns, j):
        return jnp.where(low, columns[:, 2 * j : 2 * j + 1], columns[:, 2 * j + 1 : 2 * j + 2])

    gall[me] = forget_ref[0]
    gate_cols = forget_ref[0].T
    kall[me] = k_ref[0]
    vall[me] = v_ref[0]

    inputs = (
        (x_ref, tapx_ref, slice(0, width)),
        (w_ref, tapw_ref, slice(width, width + STATE)),
        (r_ref, tapr_ref, slice(width + STATE, width + 2 * STATE)),
    )

    def filtered(count):
        for _, tap_ref, at in inputs:
            total = jnp.zeros((count, at.stop - at.start), F32)
            for i in range(taps):
                first = 8 - (taps - 1) + i
                total = total + tap_ref[i : i + 1, :].astype(F32) * pad_ref[first : first + count, at]
            conv[0:count, at] = (total * jax.nn.sigmoid(total)).astype(BF16)

    pad_ref[0:8, :] = jnp.zeros((8, pad_ref.shape[1]), F32)
    for ref, _, at in inputs:
        pad_ref[8 : 8 + rows, at] = ref[0].astype(F32)
    filtered(rows)

    head_row = lax.broadcasted_iota(jnp.int32, (heads, rows), 0)
    power = jnp.zeros((heads, rows), F32)
    for h in range(heads):
        power = jnp.where(head_row == h, shrink_ref[h], power)
    presoft = step_ref[0]
    step = jnp.maximum(presoft, 0.0) + jnp.log1p(jnp.exp(-jnp.abs(presoft)))
    log_decay = extra_ref[0] - jnp.exp(power) * step
    upper = (row_id <= col_id).astype(F32)
    cum = jnp.dot(log_decay, upper, precision=lax.Precision.HIGHEST, preferred_element_type=F32)
    cum_end = cum[:, rows - 1 : rows]
    decays = jnp.broadcast_to(jnp.exp(cum_end), (heads, LANES))

    @pl.when(me == 0)
    def _():
        state_in[...] = jnp.zeros(state_in.shape, BF16)

    end_scale = (jnp.exp(cum_end - cum) * step).T
    for j in range(pairs):
        end_wide[:, j * LANES : (j + 1) * LANES] = expand(end_scale, j)

    pl.semaphore_wait(barrier, sp - 1 + fs - 1 + 1)

    tail = [
        remote(
            ref.at[0, rows - 16 : rows, :],
            tails.at[:, at],
            tail_send.at[i],
            tail_recv.at[i],
            {"sp": lax.rem(me + 1, sp)},
        )
        for i, (ref, _, at) in enumerate(inputs)
    ]

    @pl.when(me < sp - 1)
    def _():
        for copy in tail:
            copy.start()

    def kv_copies(d, source):
        there = {"sp": lax.rem(me + d, sp)}
        return [
            remote(src, dst.at[source], kv_send.at[d, i], kv_recv.at[source, i], there)
            for i, (src, dst) in enumerate(
                ((k_ref.at[0], kall), (v_ref.at[0], vall), (gall.at[me], gall))
            )
        ]

    for d in range(1, sp):

        @pl.when(me + d < sp)
        def _(d=d):
            for copy in kv_copies(d, me):
                copy.start()

    for j in range(1, sp):

        @pl.when(j > me)
        def _(j=j):
            kall[j] = jnp.zeros(kall.shape[1:], BF16)
            vall[j] = jnp.zeros(vall.shape[1:], BF16)
            gall[j] = jnp.zeros(gall.shape[1:], F32)

    for h in range(heads):
        kv = h // repeat
        piece = (q_ref[0, :, h * HEAD_DIM : (h + 1) * HEAD_DIM].astype(F32) * HEAD_DIM**-0.5).astype(
            BF16
        )
        zero = jnp.zeros((rows, HEAD_DIM), BF16)
        parts = [piece if i == kv else zero for i in range(kv_heads)]
        qs[kv, (h % repeat) * rows : (h % repeat + 1) * rows, :] = jnp.concatenate(parts, axis=1)

    @pl.when(me > 0)
    def _():
        for copy in tail:
            copy.wait_recv()

    pad_ref[0:8, :] = jnp.where(me > 0, tails[...].astype(F32)[8:16], 0.0)
    filtered(16)
    conv_write = conv[:, width : width + STATE]
    turned_write = conv_write.astype(F32).T.astype(BF16)

    def st_copy(p):
        there = {"sp": lax.rem(me + 1, sp)}
        return remote(state_out.at[p], state_in.at[p], st_send.at[p], st_recv.at[p], there)

    for p in range(pairs):
        at = slice(p * LANES, (p + 1) * LANES)
        weighted = (conv[:, at].astype(F32) * end_wide[:, at]).astype(BF16)
        own_state[p] = jnp.dot(turned_write, weighted, preferred_element_type=F32)

        @pl.when(me == 0)
        def _(p=p):
            state_out[p] = own_state[p].astype(BF16)
            st_copy(p).start()

    for j in range(sp - 1):

        @pl.when(j < me)
        def _(j=j):
            for copy in kv_copies(1, j):
                copy.wait_recv()

    keys = kall[...].reshape(sp * rows, -1)
    values = vall[...].reshape(sp * rows, -1)
    visible = [j * rows + col_id <= me * rows + row_id for j in range(sp)]
    for kv in range(kv_heads):
        own = lane // HEAD_DIM == kv
        summed_values = jnp.where(own, values, jnp.ones_like(values))
        scores = lax.dot_general(
            qs[kv], keys, (((1,), (1,)), ((), ())), preferred_element_type=F32
        )
        outs = []
        for i in range(repeat):
            h = kv * repeat + i
            gate_col = gate_cols[:, h : h + 1]
            tiles = [
                jnp.where(
                    visible[j],
                    scores[i * rows : (i + 1) * rows, j * rows : (j + 1) * rows]
                    + (gate_col - gall[j, h : h + 1, :]),
                    NEGATIVE,
                )
                for j in range(sp)
            ]
            top = tiles[0]
            for tile in tiles[1:]:
                top = jnp.maximum(top, tile)
            top = jnp.max(top, axis=1, keepdims=True)
            probs = jnp.concatenate([jnp.exp(tile - top).astype(BF16) for tile in tiles], axis=1)
            both = jnp.dot(probs, summed_values, preferred_element_type=F32)
            turned = pltpu.roll(both, HEAD_DIM, 1)
            outs.append(both / turned if h % 2 == kv else turned / both)
        for i in range(0, repeat, 2):
            h = kv * repeat + i
            acts[0, :, h * HEAD_DIM : (h + 2) * HEAD_DIM] = jnp.where(
                low, outs[i], outs[i + 1]
            ).astype(BF16)

    def act_copy(origin, hop):
        there = origin ^ hop
        return remote(
            acts.at[origin],
            acts.at[there],
            act_send.at[there],
            act_recv.at[there],
            {"fs": f ^ hop},
        )

    def piece_copy(p, origin, hop):
        there = origin ^ hop
        ref = pieces if p < pairs else scales
        index = (lambda slot: (p, slot)) if p < pairs else (lambda slot: (slot,))
        return remote(
            ref.at[index(origin)],
            ref.at[index(there)],
            piece_send.at[p, there],
            piece_recv.at[p, there],
            {"fs": f ^ hop},
        )

    act_copy(0, 1).start()
    act_copy(0, 2).start()

    @pl.when(jnp.logical_and(me > 0, me < sp - 1))
    def _():
        for p in range(pairs):
            st_copy(p).wait_recv()
            decay = jnp.where(low, decays[2 * p : 2 * p + 1, :], decays[2 * p + 1 : 2 * p + 2, :])
            state_out[p] = (state_in[p].astype(F32) * decay + own_state[p]).astype(BF16)
            st_copy(p).start()

    exp_cum = jnp.exp(cum).T
    cum_col = cum.T
    conv_read = conv[:, width + STATE :]
    inner = lax.dot_general(
        conv_read, conv_write, (((1,), (1,)), ((), ())), preferred_element_type=F32
    )
    causal = row_id >= col_id
    for j in range(pairs):
        tile = conv[:, j * LANES : (j + 1) * LANES]
        parts = []
        for h in (2 * j, 2 * j + 1):
            gap = jnp.where(causal, cum_col[:, h : h + 1] - cum[h : h + 1, :], NEGATIVE)
            weights = (inner * (jnp.exp(gap) * step[h : h + 1, :])).astype(BF16)
            parts.append(jnp.dot(weights, tile, preferred_element_type=F32))
        bypass = jnp.where(low, bypass_ref[2 * j], bypass_ref[2 * j + 1])
        mix[:, j * LANES : (j + 1) * LANES] = (
            jnp.where(low, parts[0], parts[1]) + bypass * tile.astype(F32)
        )

    squares = []

    def piece(p):
        at = slice(p * LANES, (p + 1) * LANES)

        @pl.when(me == sp - 1)
        def _():
            st_copy(p).wait_recv()

        entered = jnp.dot(conv_read, state_in[p], preferred_element_type=F32)
        gate = gate_ref[0, :, at].astype(F32)
        u = (mix[:, at] + entered * expand(exp_cum, p)) * (gate * jax.nn.sigmoid(gate))
        squares.append(u * u)
        pieces[p, 0] = (u * gain_ref[0:1, at]).astype(BF16)
        piece_copy(p, 0, 2).start()
        piece_copy(p, 0, 1).start()
        if p == pairs - 1:
            piece_copy(p, 0, 3).start()

    def pass_on(p):
        piece_copy(p, 0, 2).wait_recv()
        piece_copy(p, 2, 1).start()

    for p in range(pairs):
        piece(p)
        if p == pairs - 1:
            total = functools.reduce(jnp.add, squares)
            ones = jnp.ones((8, LANES), F32)
            mean = (
                lax.dot_general(
                    ones,
                    total,
                    (((1,), (1,)), ((), ())),
                    precision=lax.Precision.HIGHEST,
                    preferred_element_type=F32,
                )
                / width
            )
            scales[0] = lax.rsqrt(mean + EPSILON)
            for d in range(1, fs):
                piece_copy(pairs, 0, d).start()
        if p == min(1, pairs - 1):
            act_copy(0, 1).wait_recv()
            act_copy(1, 2).start()
        if p >= 1:
            pass_on(p - 1)

    def half_copy(d):
        return remote(
            half_out.at[d], half_in.at[d], half_send.at[d], half_recv.at[d], {"tp": 1 - t}
        )

    def give(d):
        there = pl.ds(pl.multiple_of((1 - t) * half, half), half)
        half_out[d] = acc[d, there, :].astype(BF16)
        half_copy(d).start()

    def sum_copy(d):
        return remote(sums.at[d], landed.at[d], sum_send.at[d], sum_recv.at[d], {"fs": f ^ d})

    def finish(d):
        half_copy(d).wait_recv()
        here = pl.ds(pl.multiple_of(t * half, half), half)
        total = (acc[d, here, :] + half_in[d].astype(F32)).astype(BF16)
        if d:
            sums[d] = total
            sum_copy(d).start()
        else:
            out_ref[0, :, pl.ds(pl.multiple_of(f * cols, cols), cols)] = total

    cut = (pairs - 1) * LANES

    def most(d):
        first = jnp.concatenate([pieces[p, d] for p in range(pairs - 1)], axis=1)
        acc[d] = jnp.dot(acts[d], wat_ref[...], preferred_element_type=F32)
        acc_state[d] = jnp.dot(first, wst_ref[0:cut, :], preferred_element_type=F32)

    def rest(d):
        last = jnp.dot(pieces[pairs - 1, d], wst_ref[cut:, :], preferred_element_type=F32)
        acc[d] += (acc_state[d] + last) * scales[d].T[:, 0:1]
        give(d)

    for load in loads:
        load.wait()
    most(0)
    rest(0)
    act_copy(0, 2).wait_recv()
    most(2)
    act_copy(1, 2).wait_recv()
    for p in range(pairs - 1):
        piece_copy(p, 0, 1).wait_recv()
        piece_copy(p, 2, 1).wait_recv()
    most(1)
    most(3)
    for d in (2, 1, 3):
        piece_copy(pairs - 1, 0, d).wait_recv()
        piece_copy(pairs, 0, d).wait_recv()
        rest(d)
        if d == 2:
            finish(0)
    finish(2)
    finish(1)
    finish(3)
    for d in (2, 1, 3):
        sum_copy(d).wait_recv()
        out_ref[0, :, pl.ds(pl.multiple_of((f ^ d) * cols, cols), cols)] = landed[d]

    @pl.when(me < sp - 1)
    def _():
        for copy in tail + [st_copy(p) for p in range(pairs)]:
            copy.wait_send()

    for d in range(1, sp):

        @pl.when(me + d < sp)
        def _(d=d):
            for copy in kv_copies(d, me):
                copy.wait_send()

    for hop, origin in ((1, 0), (2, 0), (2, 1)):
        act_copy(origin, hop).wait_send()
    for p in range(pairs + 1):
        piece_copy(p, 0, 1).wait_send()
        piece_copy(p, 0, 2).wait_send()
        if p < pairs - 1:
            piece_copy(p, 2, 1).wait_send()
        else:
            piece_copy(p, 0, 3).wait_send()
    for d in range(fs):
        half_copy(d).wait_send()
    for d in range(1, fs):
        sum_copy(d).wait_send()


def fused(sp, fs, *args):
    x, w = args[0], args[1]
    rows, width = x.shape[1], x.shape[2]
    heads = args[4].shape[1]
    cols = args[16].shape[1]
    half = rows // 2
    args = list(args)
    args[11] = args[11].reshape(1, -1)
    args[15] = jnp.swapaxes(args[15], 1, 2)
    vmem = pl.BlockSpec(memory_space=pltpu.VMEM)
    smem = pl.BlockSpec(memory_space=pltpu.SMEM)
    far = pl.BlockSpec(memory_space=pl.ANY)
    specs = [smem if i in (6, 7) else far if i > 15 else vmem for i in range(len(args))]
    dma = pltpu.SemaphoreType.DMA
    kv_width = args[13].shape[2]
    kv_heads = kv_width // HEAD_DIM
    return pl.pallas_call(
        functools.partial(mixer_kernel, sp, fs),
        out_shape=jax.ShapeDtypeStruct((1, half, cols * fs), BF16),
        in_specs=specs,
        out_specs=vmem,
        scratch_shapes=[
            pltpu.VMEM(args[16].shape, BF16),
            pltpu.VMEM(args[17].shape, BF16),
            pltpu.SemaphoreType.DMA((2,)),
            pltpu.VMEM((8 + rows, width + 2 * STATE), F32),
            pltpu.VMEM((16, width + 2 * STATE), BF16),
            pltpu.VMEM((rows, width + 2 * STATE), BF16),
            pltpu.VMEM((rows, width), F32),
            pltpu.VMEM((sp, rows, kv_width), BF16),
            pltpu.VMEM((sp, rows, kv_width), BF16),
            pltpu.VMEM((sp, heads, rows), F32),
            pltpu.VMEM((kv_heads, heads // kv_heads * rows, kv_width), BF16),
            pltpu.VMEM((heads // 2, STATE, LANES), F32),
            pltpu.VMEM((heads // 2, STATE, LANES), BF16),
            pltpu.VMEM((heads // 2, STATE, LANES), BF16),
            pltpu.VMEM((rows, width), F32),
            pltpu.VMEM((fs, rows, width), BF16),
            pltpu.VMEM((heads // 2, fs, rows, LANES), BF16),
            pltpu.VMEM((fs, 8, rows), F32),
            pltpu.VMEM((fs, rows, cols), F32),
            pltpu.VMEM((fs, rows, cols), F32),
            pltpu.VMEM((fs, half, cols), BF16),
            pltpu.VMEM((fs, half, cols), BF16),
            pltpu.VMEM((fs, half, cols), BF16),
            pltpu.VMEM((fs, half, cols), BF16),
            dma((3,)),
            dma((3,)),
            dma((sp, 3)),
            dma((sp, 3)),
            dma((heads // 2,)),
            dma((heads // 2,)),
            dma((fs,)),
            dma((fs,)),
            dma((heads // 2 + 1, fs)),
            dma((heads // 2 + 1, fs)),
            dma((fs,)),
            dma((fs,)),
            dma((fs,)),
            dma((fs,)),
        ],
        compiler_params=pltpu.CompilerParams(collective_id=0, has_side_effects=True),
    )(*args)


def one_kernel(*args, sp, fs, tp):
    rows, width = args[0].shape[1:]
    heads = args[4].shape[1]
    return (
        1 < sp <= 8
        and fs == 4
        and tp == 2
        and rows == LANES
        and args[1].shape[2] == STATE == LANES
        and width == heads * HEAD_DIM
        and args[12].shape[2] == width
        and args[13].shape[2] == 2 * HEAD_DIM
        and heads % 4 == 0
    )


def solution(mesh):
    in_specs = (
        P("fs", "sp", "tp"),
        P("fs", "sp", "tp"),
        P("fs", "sp", "tp"),
        P("fs", "sp", "tp"),
        P("fs", "tp", "sp"),
        P("fs", "tp", "sp"),
        P("tp"),
        P("tp"),
        P(None, "tp"),
        P(None, "tp"),
        P(None, "tp"),
        P("tp"),
        P("fs", "sp", "tp"),
        P("fs", "sp", "tp"),
        P("fs", "sp", "tp"),
        P("fs", "sp", "tp"),
        P("tp", "fs"),
        P("tp", "fs"),
    )
    out_specs = P("fs", ("sp", "tp"), None)
    sp, fs, tp = (mesh.shape[name] for name in ("sp", "fs", "tp"))

    def body(*args):
        if one_kernel(*args, sp=sp, fs=fs, tp=tp):
            return fused(sp, fs, *args)
        return shards(*args)

    return jax.shard_map(body, mesh=mesh, in_specs=in_specs, out_specs=out_specs, check_vma=False)
```

profile of v0, /device:TPU:24, one launch (start us, length us, event | category | flops | bytes accessed | tf_op | source)
XLA Modules:
  0.0 37.1 jit_solution(7499171005659440678)
XLA Ops:
  0.0 35.4 %shard_map.172 = bf16[1,64,2048]{2,1,0:T(8,128)(2,1)} custom-call(bf16[1,128,512]{2,1,0:T(8,128)(2,1)} %x_ref.1, bf16[1,128,128]{2,1,0:T(8,128)(2,1)} %w_ref.1, bf16[1,128,128]{2,1,0:T(8,128)(2,1)} %r_ref.1, bf16[1,128,512]{2,1,0:T(8,128)(2,1)} %gate_ref.1, f32[1,8,128]{2,1,0:T(8,128)} %step_ref.1, f32[1,8,128]{2,1,0:T(8,128)} %extra_ref.1, f32[8]{0:T(128)} %shrink_ref.1, ...), custom_call_target="tpu_custom_call" | custom-call | tf_op jit(solution)/shard_map/pallas_call | solution.py:720
  35.4 1.7 %copy.20 = bf16[1,64,2048]{2,1,0:T(8,128)(2,1)} copy(bf16[1,64,2048]{2,1,0:T(8,128)(2,1)} %shard_map.172) | data formatting | bytes 524288
where the time goes:
time: 37.5 us; the launch traced here: 37.1 us
  Pallas kernels  35.4 us (94%)
  local copies, waits for them, and re-layouts  1.67 us (4%)
    pallas_call x1, Pallas kernels, fused(): pl.pallas_call(functools.partial(mixer_kernel, sp, fs), out_shape=jax.Sha...  35.4 us
    unnamed x1, local copies, waits for them, and re-layouts  1.67 us

commit v1 on v0

--- a/solution.py
+++ b/solution.py
@@ -247,6 +247,25 @@
 def mixer_kernel(
     sp,
     fs,
+    x_far,
+    w_far,
+    r_far,
+    gate_far,
+    step_far,
+    extra_far,
+    shrink_far,
+    bypass_far,
+    tapx_far,
+    tapw_far,
+    tapr_far,
+    gain_far,
+    q_far,
+    k_far,
+    v_far,
+    forget_far,
+    wst_far,
+    wat_far,
+    out_ref,
     x_ref,
     w_ref,
     r_ref,
@@ -263,11 +282,6 @@
     k_ref,
     v_ref,
     forget_ref,
-    wst_far,
-    wat_far,
-    out_ref,
-    wst_ref,
-    wat_ref,
     load_sem,
     pad_ref,
     tails,
@@ -280,28 +294,38 @@
     own_state,
     state_in,
     state_out,
+    side_in,
+    decay_out,
+    decay_in,
     mix,
-    acts,
-    pieces,
-    scales,
+    wst,
+    wat,
+    wst_x,
+    wat_x,
+    wst_y,
+    wat_y,
+    acts_mine,
+    acts_in,
+    pieces_mine,
+    pieces_in,
+    scales_mine,
+    scales_in,
     acc,
     acc_state,
-    half_out,
-    half_in,
-    sums,
-    landed,
+    returned,
     tail_send,
     tail_recv,
     kv_send,
     kv_recv,
     st_send,
     st_recv,
+    side_recv,
+    weight_send,
+    weight_recv,
     act_send,
     act_recv,
     piece_send,
     piece_recv,
-    half_send,
-    half_recv,
     sum_send,
     sum_recv,
 ):
@@ -315,25 +339,51 @@
     pairs = heads // 2
     taps = tapx_ref.shape[0]
     cols = wst_far.shape[1]
+    part = cols // 2
     half = rows // 2
-
-    loads = [
-        pltpu.make_async_copy(far, near, load_sem.at[i])
-        for i, (far, near) in enumerate(((wst_far, wst_ref), (wat_far, wat_ref)))
-    ]
-    for load in loads:
-        load.start()
 
     barrier = pltpu.get_barrier_semaphore()
     for d in range(1, sp):
         pl.semaphore_signal(
             barrier, inc=1, device_id={"sp": lax.rem(me + d, sp)}, device_id_type=MESH
         )
-    for d in range(1, fs):
-        pl.semaphore_signal(
-            barrier, inc=1, device_id={"fs": lax.rem(f + d, fs)}, device_id_type=MESH
-        )
+    for d in (1, 2):
+        for r in range(2):
+            pl.semaphore_signal(
+                barrier, inc=1, device_id={"fs": f ^ d, "tp": r}, device_id_type=MESH
+            )
     pl.semaphore_signal(barrier, inc=1, device_id={"tp": 1 - t}, device_id_type=MESH)
+
+    near = {
+        "x": (x_far, x_ref),
+        "w": (w_far, w_ref),
+        "r": (r_far, r_ref),
+        "tapx": (tapx_far, tapx_ref),
+        "tapw": (tapw_far, tapw_ref),
+        "tapr": (tapr_far, tapr_ref),
+        "step": (step_far, step_ref),
+        "extra": (extra_far, extra_ref),
+        "shrink": (shrink_far, shrink_ref),
+        "k": (k_far, k_ref),
+        "v": (v_far, v_ref),
+        "forget": (forget_far, forget_ref),
+        "q": (q_far, q_ref),
+        "wst": (wst_far, wst.at[t]),
+        "wat": (wat_far, wat.at[t]),
+        "gate": (gate_far, gate_ref),
+        "gain": (gain_far, gain_ref),
+        "bypass": (bypass_far, bypass_ref),
+    }
+    loads = {
+        name: pltpu.make_async_copy(far, here, load_sem.at[i])
+        for i, (name, (far, here)) in enumerate(near.items())
+    }
+    for load in loads.values():
+        load.start()
+
+    def loaded(*names):
+        for name in names:
+            loads[name].wait()
 
     def remote(src, dst, send, recv, where):
         return pltpu.make_async_remote_copy(
@@ -353,11 +403,6 @@
     def expand(columns, j):
         return jnp.where(low, columns[:, 2 * j : 2 * j + 1], columns[:, 2 * j + 1 : 2 * j + 2])
 
-    gall[me] = forget_ref[0]
-    gate_cols = forget_ref[0].T
-    kall[me] = k_ref[0]
-    vall[me] = v_ref[0]
-
     inputs = (
         (x_ref, tapx_ref, slice(0, width)),
         (w_ref, tapw_ref, slice(width, width + STATE)),
@@ -373,10 +418,12 @@
             conv[0:count, at] = (total * jax.nn.sigmoid(total)).astype(BF16)
 
     pad_ref[0:8, :] = jnp.zeros((8, pad_ref.shape[1]), F32)
+    loaded("x", "w", "r", "tapx", "tapw", "tapr")
     for ref, _, at in inputs:
         pad_ref[8 : 8 + rows, at] = ref[0].astype(F32)
     filtered(rows)
 
+    loaded("step", "extra", "shrink")
     head_row = lax.broadcasted_iota(jnp.int32, (heads, rows), 0)
     power = jnp.zeros((heads, rows), F32)
     for h in range(heads):
@@ -387,17 +434,54 @@
     upper = (row_id <= col_id).astype(F32)
     cum = jnp.dot(log_decay, upper, precision=lax.Precision.HIGHEST, preferred_element_type=F32)
     cum_end = cum[:, rows - 1 : rows]
-    decays = jnp.broadcast_to(jnp.exp(cum_end), (heads, LANES))
+    decay_out[...] = jnp.broadcast_to(jnp.exp(cum_end), (heads, LANES))
+
+    end_scale = (jnp.exp(cum_end - cum) * step).T
+    for j in range(pairs):
+        end_wide[:, j * LANES : (j + 1) * LANES] = expand(end_scale, j)
+
+    odd = lax.rem(me, 2) == 1
+    follows = me + 1 < sp
+
+    def own_states():
+        turned_write = conv[:, width : width + STATE].astype(F32).T.astype(BF16)
+        for p in range(pairs):
+            at = slice(p * LANES, (p + 1) * LANES)
+            weighted = (conv[:, at].astype(F32) * end_wide[:, at]).astype(BF16)
+            own_state[p] = jnp.dot(turned_write, weighted, preferred_element_type=F32)
+
+    def state_copy(p, hop):
+        there = {"sp": lax.rem(me + hop, sp)}
+        return remote(
+            state_out.at[p], state_in.at[p], st_send.at[p, hop - 1], st_recv.at[p], there
+        )
+
+    def side_copy(p):
+        there = {"sp": lax.rem(me + 1, sp)}
+        return remote(state_out.at[p], side_in.at[p], st_send.at[p, 0], side_recv.at[p], there)
+
+    def side_decay_copy():
+        there = {"sp": lax.rem(me + 1, sp)}
+        return remote(decay_out, decay_in, st_send.at[pairs, 0], side_recv.at[pairs], there)
+
+    def widened(decays, p):
+        return jnp.where(low, decays[2 * p : 2 * p + 1, :], decays[2 * p + 1 : 2 * p + 2, :])
 
     @pl.when(me == 0)
     def _():
         state_in[...] = jnp.zeros(state_in.shape, BF16)
-
-    end_scale = (jnp.exp(cum_end - cum) * step).T
-    for j in range(pairs):
-        end_wide[:, j * LANES : (j + 1) * LANES] = expand(end_scale, j)
-
-    pl.semaphore_wait(barrier, sp - 1 + fs - 1 + 1)
+        own_states()
+        for p in range(pairs):
+            state_out[p] = own_state[p].astype(BF16)
+
+    loaded("k", "v", "forget")
+    gall[me] = forget_ref[0]
+    gate_cols = forget_ref[0].T
+    kall[me] = k_ref[0]
+    vall[me] = v_ref[0]
+    loaded("wst", "wat")
+
+    pl.semaphore_wait(barrier, sp - 1 + 4 + 1)
 
     tail = [
         remote(
@@ -410,10 +494,15 @@
         for i, (ref, _, at) in enumerate(inputs)
     ]
 
-    @pl.when(me < sp - 1)
+    @pl.when(follows)
     def _():
         for copy in tail:
             copy.start()
+
+    @pl.when(me == 0)
+    def _():
+        for p in range(pairs):
+            state_copy(p, 1).start()
 
     def kv_copies(d, source):
         there = {"sp": lax.rem(me + d, sp)}
@@ -431,6 +520,24 @@
             for copy in kv_copies(d, me):
                 copy.start()
 
+    first, second = slice(0, part), slice(part, cols)
+    matrices = ((wst, wst_x, wst_y), (wat, wat_x, wat_y))
+
+    def weight_copy(kind, i):
+        whole, from_x, from_y = matrices[i]
+        src, dst, where = (
+            (whole.at[t], whole.at[t], {"tp": 1 - t}),
+            (whole.at[t, :, first], from_x.at[t], {"fs": f ^ 1}),
+            (whole.at[t, :, second], from_y.at[t], {"fs": f ^ 2}),
+            (from_x.at[t], from_x.at[t], {"tp": 1 - t}),
+            (from_y.at[t], from_y.at[t], {"tp": 1 - t}),
+        )[kind]
+        return remote(src, dst, weight_send.at[kind, i], weight_recv.at[kind, i], where)
+
+    for i in range(2):
+        for kind in (1, 2, 0):
+            weight_copy(kind, 1 - i).start()
+
     for j in range(1, sp):
 
         @pl.when(j > me)
@@ -439,6 +546,7 @@
             vall[j] = jnp.zeros(vall.shape[1:], BF16)
             gall[j] = jnp.zeros(gall.shape[1:], F32)
 
+    loaded("q")
     for h in range(heads):
         kv = h // repeat
         piece = (q_ref[0, :, h * HEAD_DIM : (h + 1) * HEAD_DIM].astype(F32) * HEAD_DIM**-0.5).astype(
@@ -452,25 +560,43 @@
     def _():
         for copy in tail:
             copy.wait_recv()
-
-    pad_ref[0:8, :] = jnp.where(me > 0, tails[...].astype(F32)[8:16], 0.0)
-    filtered(16)
-    conv_write = conv[:, width : width + STATE]
-    turned_write = conv_write.astype(F32).T.astype(BF16)
-
-    def st_copy(p):
-        there = {"sp": lax.rem(me + 1, sp)}
-        return remote(state_out.at[p], state_in.at[p], st_send.at[p], st_recv.at[p], there)
-
-    for p in range(pairs):
-        at = slice(p * LANES, (p + 1) * LANES)
-        weighted = (conv[:, at].astype(F32) * end_wide[:, at]).astype(BF16)
-        own_state[p] = jnp.dot(turned_write, weighted, preferred_element_type=F32)
-
-        @pl.when(me == 0)
-        def _(p=p):
+        pad_ref[0:8, :] = tails[...].astype(F32)[8:16]
+        filtered(16)
+        own_states()
+
+    @pl.when(jnp.logical_and(jnp.logical_not(odd), jnp.logical_and(me > 0, follows)))
+    def _():
+        for p in range(pairs):
             state_out[p] = own_state[p].astype(BF16)
-            st_copy(p).start()
+            side_copy(p).start()
+        side_decay_copy().start()
+
+    def entered(p):
+        @pl.when(jnp.logical_and(odd, me > 1))
+        def _():
+            if p == 0:
+                side_decay_copy().wait_recv()
+            side_copy(p).wait_recv()
+            state_in[p] = (
+                state_in[p].astype(F32) * widened(decay_in[...], p) + side_in[p].astype(F32)
+            ).astype(BF16)
+
+    relays = jnp.logical_and(odd, follows)
+
+    @pl.when(relays)
+    def _():
+        for p in range(pairs):
+            state_copy(p, 1).wait_recv()
+            entered(p)
+            state_out[p] = (
+                state_in[p].astype(F32) * widened(decay_out[...], p) + own_state[p]
+            ).astype(BF16)
+
+            @pl.when(me + 2 < sp)
+            def _(p=p):
+                state_copy(p, 2).start()
+
+            state_copy(p, 1).start()
 
     for j in range(sp - 1):
 
@@ -510,46 +636,69 @@
             turned = pltpu.roll(both, HEAD_DIM, 1)
             outs.append(both / turned if h % 2 == kv else turned / both)
         for i in range(0, repeat, 2):
-            h = kv * repeat + i
-            acts[0, :, h * HEAD_DIM : (h + 2) * HEAD_DIM] = jnp.where(
-                low, outs[i], outs[i + 1]
-            ).astype(BF16)
-
-    def act_copy(origin, hop):
-        there = origin ^ hop
-        return remote(
-            acts.at[origin],
-            acts.at[there],
-            act_send.at[there],
-            act_recv.at[there],
-            {"fs": f ^ hop},
-        )
-
-    def piece_copy(p, origin, hop):
-        there = origin ^ hop
-        ref = pieces if p < pairs else scales
-        index = (lambda slot: (p, slot)) if p < pairs else (lambda slot: (slot,))
-        return remote(
-            ref.at[index(origin)],
-            ref.at[index(there)],
-            piece_send.at[p, there],
-            piece_recv.at[p, there],
-            {"fs": f ^ hop},
-        )
-
-    act_copy(0, 1).start()
-    act_copy(0, 2).start()
-
-    @pl.when(jnp.logical_and(me > 0, me < sp - 1))
-    def _():
-        for p in range(pairs):
-            st_copy(p).wait_recv()
-            decay = jnp.where(low, decays[2 * p : 2 * p + 1, :], decays[2 * p + 1 : 2 * p + 2, :])
-            state_out[p] = (state_in[p].astype(F32) * decay + own_state[p]).astype(BF16)
-            st_copy(p).start()
-
+            at = slice((kv * repeat + i) * HEAD_DIM, (kv * repeat + i + 2) * HEAD_DIM)
+            merged = jnp.where(low, outs[i], outs[i + 1]).astype(BF16)
+            for r in range(2):
+                acts_mine[r, :, at] = merged[r * half : (r + 1) * half]
+
+    def targets(slot):
+        if slot == 0:
+            return [(1 - t, {"tp": 1 - t}, 0)]
+        return [(r, {"fs": f ^ slot, "tp": r}, r) for r in range(2)]
+
+    def act_copies(slot):
+        return [
+            remote(
+                acts_mine.at[r],
+                acts_in.at[slot, t],
+                act_send.at[slot, lanes],
+                act_recv.at[slot, t],
+                where,
+            )
+            for r, where, lanes in targets(slot)
+        ]
+
+    def act_wait(slot, source):
+        remote(
+            acts_mine.at[0],
+            acts_in.at[slot, source],
+            act_send.at[slot, 0],
+            act_recv.at[slot, source],
+            {"tp": 1 - t},
+        ).wait_recv()
+
+    def piece_copies(p, slot):
+        src, dst = (pieces_mine, pieces_in) if p < pairs else (scales_mine, scales_in)
+        return [
+            remote(
+                src.at[(r, p) if p < pairs else (r,)],
+                dst.at[(slot, t, p) if p < pairs else (slot, t)],
+                piece_send.at[p, slot, lanes],
+                piece_recv.at[p, slot, t],
+                where,
+            )
+            for r, where, lanes in targets(slot)
+        ]
+
+    def piece_wait(p, slot, source):
+        src, dst = (pieces_mine, pieces_in) if p < pairs else (scales_mine, scales_in)
+        remote(
+            src.at[(0, p) if p < pairs else (0,)],
+            dst.at[(slot, source, p) if p < pairs else (slot, source)],
+            piece_send.at[p, slot, 0],
+            piece_recv.at[p, slot, source],
+            {"tp": 1 - t},
+        ).wait_recv()
+
+    slots = (1, 2, 0)
+    for slot in slots:
+        for copy in act_copies(slot):
+            copy.start()
+
+    loaded("gate", "gain", "bypass")
     exp_cum = jnp.exp(cum).T
     cum_col = cum.T
+    conv_write = conv[:, width : width + STATE]
     conv_read = conv[:, width + STATE :]
     inner = lax.dot_general(
         conv_read, conv_write, (((1,), (1,)), ((), ())), preferred_element_type=F32
@@ -568,116 +717,166 @@
         )
 
     squares = []
-
-    def piece(p):
+    for p in range(pairs):
         at = slice(p * LANES, (p + 1) * LANES)
 
-        @pl.when(me == sp - 1)
-        def _():
-            st_copy(p).wait_recv()
-
-        entered = jnp.dot(conv_read, state_in[p], preferred_element_type=F32)
+        @pl.when(jnp.logical_and(me > 0, jnp.logical_not(relays)))
+        def _(p=p):
+            state_copy(p, 1).wait_recv()
+            entered(p)
+
+        carried = jnp.dot(conv_read, state_in[p], preferred_element_type=F32)
         gate = gate_ref[0, :, at].astype(F32)
-        u = (mix[:, at] + entered * expand(exp_cum, p)) * (gate * jax.nn.sigmoid(gate))
+        u = (mix[:, at] + carried * expand(exp_cum, p)) * (gate * jax.nn.sigmoid(gate))
         squares.append(u * u)
-        pieces[p, 0] = (u * gain_ref[0:1, at]).astype(BF16)
-        piece_copy(p, 0, 2).start()
-        piece_copy(p, 0, 1).start()
-        if p == pairs - 1:
-            piece_copy(p, 0, 3).start()
-
-    def pass_on(p):
-        piece_copy(p, 0, 2).wait_recv()
-        piece_copy(p, 2, 1).start()
-
+        sent = (u * gain_ref[0:1, at]).astype(BF16)
+        for r in range(2):
+            pieces_mine[r, p] = sent[r * half : (r + 1) * half]
+        for slot in slots:
+            for copy in piece_copies(p, slot):
+                copy.start()
+
+    total = functools.reduce(jnp.add, squares)
+    mean = (
+        lax.dot_general(
+            jnp.ones((8, LANES), F32),
+            total,
+            (((1,), (1,)), ((), ())),
+            precision=lax.Precision.HIGHEST,
+            preferred_element_type=F32,
+        )
+        / width
+    )
+    scale = lax.rsqrt(mean + EPSILON)
+    scales_mine[0] = scale
+    scales_mine[1] = pltpu.roll(scale, half, 1)
+    for slot in slots:
+        for copy in piece_copies(pairs, slot):
+            copy.start()
+
+    acts_in[0, t] = acts_mine[t]
     for p in range(pairs):
-        piece(p)
-        if p == pairs - 1:
-            total = functools.reduce(jnp.add, squares)
-            ones = jnp.ones((8, LANES), F32)
-            mean = (
-                lax.dot_general(
-                    ones,
-                    total,
-                    (((1,), (1,)), ((), ())),
-                    precision=lax.Precision.HIGHEST,
-                    preferred_element_type=F32,
-                )
-                / width
+        pieces_in[0, t, p] = pieces_mine[t, p]
+    scales_in[0, t] = scales_mine[t]
+
+    for i in (1, 0):
+        for kind in (1, 2):
+            weight_copy(kind, i).wait_recv()
+            weight_copy(kind + 2, i).start()
+
+    groups = (
+        (2, wst, wat, first),
+        (2, wst_x, wat_x, slice(0, part)),
+        (1, wst, wat, second),
+        (1, wst_y, wat_y, slice(0, part)),
+    )
+    needs = (0, 3, 0, 4)
+
+    def from_peer(kind, i):
+        whole, from_x, from_y = matrices[i]
+        ref = (whole, None, None, from_x, from_y)[kind]
+        remote(
+            ref.at[1 - t],
+            ref.at[1 - t],
+            weight_send.at[kind, i],
+            weight_recv.at[kind, i],
+            {"tp": 1 - t},
+        ).wait_recv()
+
+    act_wait(0, 1 - t)
+    for slot in (2, 1):
+        for source in range(2):
+            act_wait(slot, source)
+    for kind in (0, 3, 4):
+        from_peer(kind, 1)
+    for g, (slot, _, weights, at) in enumerate(groups):
+        left = jnp.concatenate(
+            [
+                jnp.concatenate([acts_in[0, s], acts_in[slot, s]], axis=0)
+                for s in range(2)
+            ],
+            axis=1,
+        )
+        right = jnp.concatenate([weights[s, :, at] for s in range(2)], axis=0)
+        acc[g] = jnp.dot(left, right, preferred_element_type=F32)
+
+    for kind in (0, 3, 4):
+        from_peer(kind, 0)
+    for p in range(pairs - 1):
+        piece_wait(p, 0, 1 - t)
+        for slot in (2, 1):
+            for source in range(2):
+                piece_wait(p, slot, source)
+
+    cut = (pairs - 1) * LANES
+
+    def stacked(slot, s, p):
+        return jnp.concatenate([pieces_in[0, s, p], pieces_in[slot, s, p]], axis=0)
+
+    for g, (slot, weights, _, at) in enumerate(groups):
+        for s in range(2):
+            left = jnp.concatenate([stacked(slot, s, p) for p in range(pairs - 1)], axis=1)
+            acc_state[g, s] = jnp.dot(left, weights[s, 0:cut, at], preferred_element_type=F32)
+
+    for p in (pairs - 1, pairs):
+        piece_wait(p, 0, 1 - t)
+        for slot in (2, 1):
+            for source in range(2):
+                piece_wait(p, slot, source)
+
+    def columns(owner, at):
+        return pl.ds(pl.multiple_of(owner * cols + at.start, part), part)
+
+    def sum_copy(g):
+        slot = groups[g][0]
+        owner = (f, f ^ 1, f, f ^ 2)[g]
+        at = (first, first, second, second)[g]
+        return remote(
+            returned.at[g],
+            out_ref.at[0, :, columns(owner, at)],
+            sum_send.at[g],
+            sum_recv.at[g],
+            {"fs": f ^ slot},
+        )
+
+    turned = [[scales_in[slot, s].T[0:half, 0:1] for s in range(2)] for slot in range(3)]
+    for g, (slot, weights, _, at) in enumerate(groups):
+        merged = acc[g]
+        for s in range(2):
+            last = jnp.dot(
+                stacked(slot, s, pairs - 1), weights[s, cut:, at], preferred_element_type=F32
             )
-            scales[0] = lax.rsqrt(mean + EPSILON)
-            for d in range(1, fs):
-                piece_copy(pairs, 0, d).start()
-        if p == min(1, pairs - 1):
-            act_copy(0, 1).wait_recv()
-            act_copy(1, 2).start()
-        if p >= 1:
-            pass_on(p - 1)
-
-    def half_copy(d):
-        return remote(
-            half_out.at[d], half_in.at[d], half_send.at[d], half_recv.at[d], {"tp": 1 - t}
-        )
-
-    def give(d):
-        there = pl.ds(pl.multiple_of((1 - t) * half, half), half)
-        half_out[d] = acc[d, there, :].astype(BF16)
-        half_copy(d).start()
-
-    def sum_copy(d):
-        return remote(sums.at[d], landed.at[d], sum_send.at[d], sum_recv.at[d], {"fs": f ^ d})
-
-    def finish(d):
-        half_copy(d).wait_recv()
-        here = pl.ds(pl.multiple_of(t * half, half), half)
-        total = (acc[d, here, :] + half_in[d].astype(F32)).astype(BF16)
-        if d:
-            sums[d] = total
-            sum_copy(d).start()
-        else:
-            out_ref[0, :, pl.ds(pl.multiple_of(f * cols, cols), cols)] = total
-
-    cut = (pairs - 1) * LANES
-
-    def most(d):
-        first = jnp.concatenate([pieces[p, d] for p in range(pairs - 1)], axis=1)
-        acc[d] = jnp.dot(acts[d], wat_ref[...], preferred_element_type=F32)
-        acc_state[d] = jnp.dot(first, wst_ref[0:cut, :], preferred_element_type=F32)
-
-    def rest(d):
-        last = jnp.dot(pieces[pairs - 1, d], wst_ref[cut:, :], preferred_element_type=F32)
-        acc[d] += (acc_state[d] + last) * scales[d].T[:, 0:1]
-        give(d)
-
-    for load in loads:
-        load.wait()
-    most(0)
-    rest(0)
-    act_copy(0, 2).wait_recv()
-    most(2)
-    act_copy(1, 2).wait_recv()
-    for p in range(pairs - 1):
-        piece_copy(p, 0, 1).wait_recv()
-        piece_copy(p, 2, 1).wait_recv()
-    most(1)
-    most(3)
-    for d in (2, 1, 3):
-        piece_copy(pairs - 1, 0, d).wait_recv()
-        piece_copy(pairs, 0, d).wait_recv()
-        rest(d)
-        if d == 2:
-            finish(0)
-    finish(2)
-    finish(1)
-    finish(3)
-    for d in (2, 1, 3):
-        sum_copy(d).wait_recv()
-        out_ref[0, :, pl.ds(pl.multiple_of((f ^ d) * cols, cols), cols)] = landed[d]
-
-    @pl.when(me < sp - 1)
+            by = jnp.concatenate([turned[0][s], turned[slot][s]], axis=0)
+            merged = merged + (acc_state[g, s] + last) * by
+        merged = merged.astype(BF16)
+        returned[g] = merged[half:]
+        sum_copy(g).start()
+        owner = (f, f ^ 1, f, f ^ 2)[g]
+        out_ref[0, :, columns(owner, (first, first, second, second)[g])] = merged[0:half]
+
+    for g in range(4):
+        sum_copy(g).wait_recv()
+
+    @pl.when(follows)
     def _():
-        for copy in tail + [st_copy(p) for p in range(pairs)]:
+        for copy in tail:
             copy.wait_send()
+
+    @pl.when(jnp.logical_and(follows, jnp.logical_or(odd, me == 0)))
+    def _():
+        for p in range(pairs):
+            state_copy(p, 1).wait_send()
+
+    @pl.when(jnp.logical_and(odd, me + 2 < sp))
+    def _():
+        for p in range(pairs):
+            state_copy(p, 2).wait_send()
+
+    @pl.when(jnp.logical_and(jnp.logical_not(odd), jnp.logical_and(me > 0, follows)))
+    def _():
+        for p in range(pairs):
+            side_copy(p).wait_send()
+        side_decay_copy().wait_send()
 
     for d in range(1, sp):
 
@@ -686,46 +885,45 @@
             for copy in kv_copies(d, me):
                 copy.wait_send()
 
-    for hop, origin in ((1, 0), (2, 0), (2, 1)):
-        act_copy(origin, hop).wait_send()
-    for p in range(pairs + 1):
-        piece_copy(p, 0, 1).wait_send()
-        piece_copy(p, 0, 2).wait_send()
-        if p < pairs - 1:
-            piece_copy(p, 2, 1).wait_send()
-        else:
-            piece_copy(p, 0, 3).wait_send()
-    for d in range(fs):
-        half_copy(d).wait_send()
-    for d in range(1, fs):
-        sum_copy(d).wait_send()
+    for kind in range(5):
+        for i in range(2):
+            weight_copy(kind, i).wait_send()
+    for slot in slots:
+        for copy in act_copies(slot):
+            copy.wait_send()
+        for p in range(pairs + 1):
+            for copy in piece_copies(p, slot):
+                copy.wait_send()
+    for g in range(4):
+        sum_copy(g).wait_send()
 
 
 def fused(sp, fs, *args):
-    x, w = args[0], args[1]
-    rows, width = x.shape[1], x.shape[2]
+    rows, width = args[0].shape[1:]
     heads = args[4].shape[1]
-    cols = args[16].shape[1]
-    half = rows // 2
+    deep, cols = args[16].shape
+    half, part = rows // 2, cols // 2
     args = list(args)
     args[11] = args[11].reshape(1, -1)
     args[15] = jnp.swapaxes(args[15], 1, 2)
     vmem = pl.BlockSpec(memory_space=pltpu.VMEM)
-    smem = pl.BlockSpec(memory_space=pltpu.SMEM)
     far = pl.BlockSpec(memory_space=pl.ANY)
-    specs = [smem if i in (6, 7) else far if i > 15 else vmem for i in range(len(args))]
     dma = pltpu.SemaphoreType.DMA
     kv_width = args[13].shape[2]
     kv_heads = kv_width // HEAD_DIM
+    pairs = heads // 2
+    near = [
+        (pltpu.SMEM if i in (6, 7) else pltpu.VMEM)(a.shape, a.dtype)
+        for i, a in enumerate(args[:16])
+    ]
     return pl.pallas_call(
         functools.partial(mixer_kernel, sp, fs),
         out_shape=jax.ShapeDtypeStruct((1, half, cols * fs), BF16),
-        in_specs=specs,
+        in_specs=[far] * len(args),
         out_specs=vmem,
-        scratch_shapes=[
-            pltpu.VMEM(args[16].shape, BF16),
-            pltpu.VMEM(args[17].shape, BF16),
-            pltpu.SemaphoreType.DMA((2,)),
+        scratch_shapes=near
+        + [
+            dma((len(args),)),
             pltpu.VMEM((8 + rows, width + 2 * STATE), F32),
             pltpu.VMEM((16, width + 2 * STATE), BF16),
             pltpu.VMEM((rows, width + 2 * STATE), BF16),
@@ -734,33 +932,43 @@
             pltpu.VMEM((sp, rows, kv_width), BF16),
             pltpu.VMEM((sp, heads, rows), F32),
             pltpu.VMEM((kv_heads, heads // kv_heads * rows, kv_width), BF16),
-            pltpu.VMEM((heads // 2, STATE, LANES), F32),
-            pltpu.VMEM((heads // 2, STATE, LANES), BF16),
-            pltpu.VMEM((heads // 2, STATE, LANES), BF16),
+            pltpu.VMEM((pairs, STATE, LANES), F32),
+            pltpu.VMEM((pairs, STATE, LANES), BF16),
+            pltpu.VMEM((pairs, STATE, LANES), BF16),
+            pltpu.VMEM((pairs, STATE, LANES), BF16),
+            pltpu.VMEM((heads, LANES), F32),
+            pltpu.VMEM((heads, LANES), F32),
             pltpu.VMEM((rows, width), F32),
-            pltpu.VMEM((fs, rows, width), BF16),
-            pltpu.VMEM((heads // 2, fs, rows, LANES), BF16),
-            pltpu.VMEM((fs, 8, rows), F32),
-            pltpu.VMEM((fs, rows, cols), F32),
-            pltpu.VMEM((fs, rows, cols), F32),
-            pltpu.VMEM((fs, half, cols), BF16),
-            pltpu.VMEM((fs, half, cols), BF16),
-            pltpu.VMEM((fs, half, cols), BF16),
-            pltpu.VMEM((fs, half, cols), BF16),
+            pltpu.VMEM((2, deep, cols), BF16),
+            pltpu.VMEM((2, deep, cols), BF16),
+            pltpu.VMEM((2, deep, part), BF16),
+            pltpu.VMEM((2, deep, part), BF16),
+            pltpu.VMEM((2, deep, part), BF16),
+            pltpu.VMEM((2, deep, part), BF16),
+            pltpu.VMEM((2, half, width), BF16),
+            pltpu.VMEM((3, 2, half, width), BF16),
+            pltpu.VMEM((2, pairs, half, LANES), BF16),
+            pltpu.VMEM((3, 2, pairs, half, LANES), BF16),
+            pltpu.VMEM((2, 8, rows), F32),
+            pltpu.VMEM((3, 2, 8, rows), F32),
+            pltpu.VMEM((4, rows, part), F32),
+            pltpu.VMEM((4, 2, rows, part), F32),
+            pltpu.VMEM((4, half, part), BF16),
             dma((3,)),
             dma((3,)),
             dma((sp, 3)),
             dma((sp, 3)),
-            dma((heads // 2,)),
-            dma((heads // 2,)),
-            dma((fs,)),
-            dma((fs,)),
-            dma((heads // 2 + 1, fs)),
-            dma((heads // 2 + 1, fs)),
-            dma((fs,)),
-            dma((fs,)),
-            dma((fs,)),
-            dma((fs,)),
+            dma((pairs + 1, 2)),
+            dma((pairs,)),
+            dma((pairs + 1,)),
+            dma((5, 2)),
+            dma((5, 2)),
+            dma((3, 2)),
+            dma((3, 2)),
+            dma((pairs + 1, 3, 2)),
+            dma((pairs + 1, 3, 2)),
+            dma((4,)),
+            dma((4,)),
         ],
         compiler_params=pltpu.CompilerParams(collective_id=0, has_side_effects=True),
     )(*args)
@@ -779,6 +987,8 @@
         and args[12].shape[2] == width
         and args[13].shape[2] == 2 * HEAD_DIM
         and heads % 4 == 0
+        and args[16].shape == args[17].shape == (width, args[16].shape[1])
+        and args[16].shape[1] % (2 * LANES) == 0
     )
 
 

time: 37.5 us -> 32.5 us (0.87)
  the two profiles are of different devices: /device:TPU:24 before, /device:TPU:0 now
where the time goes in v1:
time: 32.5 us; the launch traced here: 32.4 us
  Pallas kernels  30.7 us (94%)
  local copies, waits for them, and re-layouts  1.67 us (5%)
    pallas_call x1, Pallas kernels, fused(): pl.pallas_call(functools.partial(mixer_kernel, sp, fs), out_shape=jax.Sha...  30.7 us
    unnamed x1, local copies, waits for them, and re-layouts  1.67 us

profile of v1, /device:TPU:0, one launch (start us, length us, event | category | flops | bytes accessed | tf_op | source)
XLA Modules:
  0.0 32.4 jit_solution(1088411709729749314)
XLA Ops:
  0.0 30.7 %shard_map.172 = bf16[1,64,2048]{2,1,0:T(8,128)(2,1)} custom-call(bf16[1,128,512]{2,1,0:T(8,128)(2,1)} %x_far.1, bf16[1,128,128]{2,1,0:T(8,128)(2,1)} %w_far.1, bf16[1,128,128]{2,1,0:T(8,128)(2,1)} %r_far.1, bf16[1,128,512]{2,1,0:T(8,128)(2,1)} %gate_far.1, f32[1,8,128]{2,1,0:T(8,128)} %step_far.1, f32[1,8,128]{2,1,0:T(8,128)} %extra_far.1, f32[8]{0:T(128)} %shrink_far.1, ...), custom_call_target="tpu_custom_call" | custom-call | tf_op jit(solution)/shard_map/pallas_call | solution.py:919
  30.7 1.7 %copy.20 = bf16[1,64,2048]{2,1,0:T(8,128)(2,1)} copy(bf16[1,64,2048]{2,1,0:T(8,128)(2,1)} %shard_map.172) | data formatting | bytes 524288

commit v2 on v1

--- a/solution.py
+++ b/solution.py
@@ -279,31 +279,24 @@
     tapr_ref,
     gain_ref,
     q_ref,
-    k_ref,
-    v_ref,
     forget_ref,
     load_sem,
+    ready,
     pad_ref,
     tails,
     conv,
     end_wide,
-    kall,
-    vall,
+    kvall,
     gall,
     qs,
     own_state,
     state_in,
     state_out,
-    side_in,
-    decay_out,
-    decay_in,
     mix,
     wst,
     wat,
-    wst_x,
+    wst_y,
     wat_x,
-    wst_y,
-    wat_y,
     acts_mine,
     acts_in,
     pieces_mine,
@@ -312,18 +305,17 @@
     scales_in,
     acc,
     acc_state,
-    returned,
-    tail_send,
-    tail_recv,
-    kv_send,
-    kv_recv,
+    att_out,
+    att_in,
+    sum_out,
+    sum_in,
+    tail_sem,
+    kv_sem,
     st_send,
     st_recv,
-    side_recv,
     weight_send,
     weight_recv,
-    act_send,
-    act_recv,
+    act_sem,
     piece_send,
     piece_recv,
     sum_send,
@@ -334,25 +326,28 @@
     t = lax.axis_index("tp")
     rows, width = x_ref.shape[1], x_ref.shape[2]
     heads = step_ref.shape[1]
-    kv_heads = k_ref.shape[2] // HEAD_DIM
+    kv_width = k_far.shape[2]
+    kv_heads = kv_width // HEAD_DIM
     repeat = heads // kv_heads
     pairs = heads // 2
     taps = tapx_ref.shape[0]
     cols = wst_far.shape[1]
     part = cols // 2
     half = rows // 2
+    peer = {"tp": 1 - t}
 
     barrier = pltpu.get_barrier_semaphore()
-    for d in range(1, sp):
-        pl.semaphore_signal(
-            barrier, inc=1, device_id={"sp": lax.rem(me + d, sp)}, device_id_type=MESH
-        )
     for d in (1, 2):
         for r in range(2):
             pl.semaphore_signal(
                 barrier, inc=1, device_id={"fs": f ^ d, "tp": r}, device_id_type=MESH
             )
-    pl.semaphore_signal(barrier, inc=1, device_id={"tp": 1 - t}, device_id_type=MESH)
+    pl.semaphore_signal(barrier, inc=1, device_id=peer, device_id_type=MESH)
+    for d in range(1, sp):
+
+        @pl.when(me + d < sp)
+        def _(d=d):
+            pl.semaphore_signal(barrier, inc=1, device_id={"sp": me + d}, device_id_type=MESH)
 
     near = {
         "x": (x_far, x_ref),
@@ -361,15 +356,15 @@
         "tapx": (tapx_far, tapx_ref),
         "tapw": (tapw_far, tapw_ref),
         "tapr": (tapr_far, tapr_ref),
+        "k": (k_far.at[0], kvall.at[me, :, 0:kv_width]),
+        "v": (v_far.at[0], kvall.at[me, :, kv_width:]),
+        "wat": (wat_far, wat.at[t]),
+        "wst": (wst_far, wst.at[t]),
         "step": (step_far, step_ref),
         "extra": (extra_far, extra_ref),
         "shrink": (shrink_far, shrink_ref),
-        "k": (k_far, k_ref),
-        "v": (v_far, v_ref),
         "forget": (forget_far, forget_ref),
         "q": (q_far, q_ref),
-        "wst": (wst_far, wst.at[t]),
-        "wat": (wat_far, wat.at[t]),
         "gate": (gate_far, gate_ref),
         "gain": (gain_far, gain_ref),
         "bypass": (bypass_far, bypass_ref),
@@ -395,6 +390,12 @@
             device_id_type=MESH,
         )
 
+    def arrived(ref, sem):
+        remote(ref, ref, sem, sem, peer).wait_recv()
+
+    def departed(ref, sem):
+        remote(ref, ref, sem, sem, peer).wait_send()
+
     lane = lax.broadcasted_iota(jnp.int32, (1, LANES), 1)
     low = lane < HEAD_DIM
     row_id = lax.broadcasted_iota(jnp.int32, (rows, rows), 0)
@@ -422,6 +423,37 @@
     for ref, _, at in inputs:
         pad_ref[8 : 8 + rows, at] = ref[0].astype(F32)
     filtered(rows)
+
+    loaded("wat", "wst")
+    pl.semaphore_wait(barrier, 5 + me)
+
+    def weight_copies(kind):
+        return (
+            (
+                remote(wat.at[t], wat_x.at[t], weight_send.at[0], weight_recv.at[0], {"fs": f ^ 1}),
+                remote(wst.at[t], wst_y.at[t], weight_send.at[0], weight_recv.at[1], {"fs": f ^ 2}),
+            ),
+            (
+                remote(wat.at[t], wat.at[t], weight_send.at[1], weight_recv.at[2], peer),
+                remote(wst.at[t], wst.at[t], weight_send.at[1], weight_recv.at[3], peer),
+            ),
+            (
+                remote(wat_x.at[t], wat_x.at[t], weight_send.at[2], weight_recv.at[2], peer),
+                remote(wst_y.at[t], wst_y.at[t], weight_send.at[2], weight_recv.at[3], peer),
+            ),
+        )[kind]
+
+    for kind in range(2):
+        for copy in weight_copies(kind):
+            copy.start()
+
+    for d in range(1, sp):
+
+        @pl.when(me - d >= 0)
+        def _(d=d):
+            pl.semaphore_signal(
+                ready.at[d - 1], inc=1, device_id={"sp": me - d}, device_id_type=MESH
+            )
 
     loaded("step", "extra", "shrink")
     head_row = lax.broadcasted_iota(jnp.int32, (heads, rows), 0)
@@ -434,13 +466,12 @@
     upper = (row_id <= col_id).astype(F32)
     cum = jnp.dot(log_decay, upper, precision=lax.Precision.HIGHEST, preferred_element_type=F32)
     cum_end = cum[:, rows - 1 : rows]
-    decay_out[...] = jnp.broadcast_to(jnp.exp(cum_end), (heads, LANES))
+    decays = jnp.broadcast_to(jnp.exp(cum_end), (heads, LANES))
 
     end_scale = (jnp.exp(cum_end - cum) * step).T
     for j in range(pairs):
         end_wide[:, j * LANES : (j + 1) * LANES] = expand(end_scale, j)
 
-    odd = lax.rem(me, 2) == 1
     follows = me + 1 < sp
 
     def own_states():
@@ -450,22 +481,9 @@
             weighted = (conv[:, at].astype(F32) * end_wide[:, at]).astype(BF16)
             own_state[p] = jnp.dot(turned_write, weighted, preferred_element_type=F32)
 
-    def state_copy(p, hop):
-        there = {"sp": lax.rem(me + hop, sp)}
-        return remote(
-            state_out.at[p], state_in.at[p], st_send.at[p, hop - 1], st_recv.at[p], there
-        )
-
-    def side_copy(p):
+    def state_copy(p):
         there = {"sp": lax.rem(me + 1, sp)}
-        return remote(state_out.at[p], side_in.at[p], st_send.at[p, 0], side_recv.at[p], there)
-
-    def side_decay_copy():
-        there = {"sp": lax.rem(me + 1, sp)}
-        return remote(decay_out, decay_in, st_send.at[pairs, 0], side_recv.at[pairs], there)
-
-    def widened(decays, p):
-        return jnp.where(low, decays[2 * p : 2 * p + 1, :], decays[2 * p + 1 : 2 * p + 2, :])
+        return remote(state_out.at[p], state_in.at[p], st_send, st_recv.at[p], there)
 
     @pl.when(me == 0)
     def _():
@@ -477,73 +495,50 @@
     loaded("k", "v", "forget")
     gall[me] = forget_ref[0]
     gate_cols = forget_ref[0].T
-    kall[me] = k_ref[0]
-    vall[me] = v_ref[0]
-    loaded("wst", "wat")
-
-    pl.semaphore_wait(barrier, sp - 1 + 4 + 1)
 
     tail = [
         remote(
             ref.at[0, rows - 16 : rows, :],
             tails.at[:, at],
-            tail_send.at[i],
-            tail_recv.at[i],
+            tail_sem.at[0],
+            tail_sem.at[1],
             {"sp": lax.rem(me + 1, sp)},
         )
-        for i, (ref, _, at) in enumerate(inputs)
+        for ref, _, at in inputs
     ]
+
+    def kv_copies(d):
+        there = {"sp": lax.rem(me + d, sp)}
+        return [
+            remote(kvall.at[me], kvall.at[me], kv_sem.at[0], kv_sem.at[1], there),
+            remote(gall.at[me], gall.at[me], kv_sem.at[2], kv_sem.at[3], there),
+        ]
 
     @pl.when(follows)
     def _():
+        pl.semaphore_wait(ready.at[0], 1)
         for copy in tail:
             copy.start()
 
     @pl.when(me == 0)
     def _():
         for p in range(pairs):
-            state_copy(p, 1).start()
-
-    def kv_copies(d, source):
-        there = {"sp": lax.rem(me + d, sp)}
-        return [
-            remote(src, dst.at[source], kv_send.at[d, i], kv_recv.at[source, i], there)
-            for i, (src, dst) in enumerate(
-                ((k_ref.at[0], kall), (v_ref.at[0], vall), (gall.at[me], gall))
-            )
-        ]
+            state_copy(p).start()
 
     for d in range(1, sp):
 
         @pl.when(me + d < sp)
         def _(d=d):
-            for copy in kv_copies(d, me):
+            if d > 1:
+                pl.semaphore_wait(ready.at[d - 1], 1)
+            for copy in kv_copies(d):
                 copy.start()
-
-    first, second = slice(0, part), slice(part, cols)
-    matrices = ((wst, wst_x, wst_y), (wat, wat_x, wat_y))
-
-    def weight_copy(kind, i):
-        whole, from_x, from_y = matrices[i]
-        src, dst, where = (
-            (whole.at[t], whole.at[t], {"tp": 1 - t}),
-            (whole.at[t, :, first], from_x.at[t], {"fs": f ^ 1}),
-            (whole.at[t, :, second], from_y.at[t], {"fs": f ^ 2}),
-            (from_x.at[t], from_x.at[t], {"tp": 1 - t}),
-            (from_y.at[t], from_y.at[t], {"tp": 1 - t}),
-        )[kind]
-        return remote(src, dst, weight_send.at[kind, i], weight_recv.at[kind, i], where)
-
-    for i in range(2):
-        for kind in (1, 2, 0):
-            weight_copy(kind, 1 - i).start()
 
     for j in range(1, sp):
 
         @pl.when(j > me)
         def _(j=j):
-            kall[j] = jnp.zeros(kall.shape[1:], BF16)
-            vall[j] = jnp.zeros(vall.shape[1:], BF16)
+            kvall[j] = jnp.zeros(kvall.shape[1:], BF16)
             gall[j] = jnp.zeros(gall.shape[1:], F32)
 
     loaded("q")
@@ -556,57 +551,63 @@
         parts = [piece if i == kv else zero for i in range(kv_heads)]
         qs[kv, (h % repeat) * rows : (h % repeat + 1) * rows, :] = jnp.concatenate(parts, axis=1)
 
+    loaded("gate", "gain", "bypass")
+    exp_cum = jnp.exp(cum).T
+    cum_col = cum.T
+
+    def within():
+        conv_write = conv[:, width : width + STATE]
+        conv_read = conv[:, width + STATE :]
+        inner = lax.dot_general(
+            conv_read, conv_write, (((1,), (1,)), ((), ())), preferred_element_type=F32
+        )
+        causal = row_id >= col_id
+        for j in range(pairs):
+            tile = conv[:, j * LANES : (j + 1) * LANES]
+            parts = []
+            for h in (2 * j, 2 * j + 1):
+                gap = jnp.where(causal, cum_col[:, h : h + 1] - cum[h : h + 1, :], NEGATIVE)
+                weights = (inner * (jnp.exp(gap) * step[h : h + 1, :])).astype(BF16)
+                parts.append(jnp.dot(weights, tile, preferred_element_type=F32))
+            bypass = jnp.where(low, bypass_ref[2 * j], bypass_ref[2 * j + 1])
+            mix[:, j * LANES : (j + 1) * LANES] = (
+                jnp.where(low, parts[0], parts[1]) + bypass * tile.astype(F32)
+            )
+
     @pl.when(me > 0)
     def _():
-        for copy in tail:
-            copy.wait_recv()
+        arrived(tails, tail_sem.at[1])
         pad_ref[0:8, :] = tails[...].astype(F32)[8:16]
         filtered(16)
         own_states()
 
-    @pl.when(jnp.logical_and(jnp.logical_not(odd), jnp.logical_and(me > 0, follows)))
+    @pl.when(me != 1)
     def _():
-        for p in range(pairs):
-            state_out[p] = own_state[p].astype(BF16)
-            side_copy(p).start()
-        side_decay_copy().start()
-
-    def entered(p):
-        @pl.when(jnp.logical_and(odd, me > 1))
-        def _():
-            if p == 0:
-                side_decay_copy().wait_recv()
-            side_copy(p).wait_recv()
-            state_in[p] = (
-                state_in[p].astype(F32) * widened(decay_in[...], p) + side_in[p].astype(F32)
-            ).astype(BF16)
-
-    relays = jnp.logical_and(odd, follows)
+        within()
+
+    relays = jnp.logical_and(me > 0, follows)
 
     @pl.when(relays)
     def _():
         for p in range(pairs):
-            state_copy(p, 1).wait_recv()
-            entered(p)
-            state_out[p] = (
-                state_in[p].astype(F32) * widened(decay_out[...], p) + own_state[p]
-            ).astype(BF16)
-
-            @pl.when(me + 2 < sp)
-            def _(p=p):
-                state_copy(p, 2).start()
-
-            state_copy(p, 1).start()
-
-    for j in range(sp - 1):
-
-        @pl.when(j < me)
+            state_copy(p).wait_recv()
+            decay = jnp.where(low, decays[2 * p : 2 * p + 1, :], decays[2 * p + 1 : 2 * p + 2, :])
+            state_out[p] = (state_in[p].astype(F32) * decay + own_state[p]).astype(BF16)
+            state_copy(p).start()
+
+    @pl.when(me == 1)
+    def _():
+        within()
+
+    for j in range(1, sp):
+
+        @pl.when(me == j)
         def _(j=j):
-            for copy in kv_copies(1, j):
-                copy.wait_recv()
-
-    keys = kall[...].reshape(sp * rows, -1)
-    values = vall[...].reshape(sp * rows, -1)
+            arrived(kvall.at[0:j], kv_sem.at[1])
+            arrived(gall.at[0:j], kv_sem.at[3])
+
+    keys = kvall[:, :, 0:kv_width].reshape(sp * rows, -1)
+    values = kvall[:, :, kv_width:].reshape(sp * rows, -1)
     visible = [j * rows + col_id <= me * rows + row_id for j in range(sp)]
     for kv in range(kv_heads):
         own = lane // HEAD_DIM == kv
@@ -641,89 +642,23 @@
             for r in range(2):
                 acts_mine[r, :, at] = merged[r * half : (r + 1) * half]
 
-    def targets(slot):
-        if slot == 0:
-            return [(1 - t, {"tp": 1 - t}, 0)]
-        return [(r, {"fs": f ^ slot, "tp": r}, r) for r in range(2)]
-
-    def act_copies(slot):
+    def spread(src, dst, send, recv, hop):
         return [
-            remote(
-                acts_mine.at[r],
-                acts_in.at[slot, t],
-                act_send.at[slot, lanes],
-                act_recv.at[slot, t],
-                where,
-            )
-            for r, where, lanes in targets(slot)
-        ]
-
-    def act_wait(slot, source):
-        remote(
-            acts_mine.at[0],
-            acts_in.at[slot, source],
-            act_send.at[slot, 0],
-            act_recv.at[slot, source],
-            {"tp": 1 - t},
-        ).wait_recv()
-
-    def piece_copies(p, slot):
-        src, dst = (pieces_mine, pieces_in) if p < pairs else (scales_mine, scales_in)
-        return [
-            remote(
-                src.at[(r, p) if p < pairs else (r,)],
-                dst.at[(slot, t, p) if p < pairs else (slot, t)],
-                piece_send.at[p, slot, lanes],
-                piece_recv.at[p, slot, t],
-                where,
-            )
-            for r, where, lanes in targets(slot)
-        ]
-
-    def piece_wait(p, slot, source):
-        src, dst = (pieces_mine, pieces_in) if p < pairs else (scales_mine, scales_in)
-        remote(
-            src.at[(0, p) if p < pairs else (0,)],
-            dst.at[(slot, source, p) if p < pairs else (slot, source)],
-            piece_send.at[p, slot, 0],
-            piece_recv.at[p, slot, source],
-            {"tp": 1 - t},
-        ).wait_recv()
-
-    slots = (1, 2, 0)
-    for slot in slots:
-        for copy in act_copies(slot):
-            copy.start()
-
-    loaded("gate", "gain", "bypass")
-    exp_cum = jnp.exp(cum).T
-    cum_col = cum.T
-    conv_write = conv[:, width : width + STATE]
+            remote(src.at[r], dst.at[2 + t], send, recv, {"fs": f ^ hop, "tp": r})
+            for r in range(2)
+        ] + [remote(src.at[1 - t], dst.at[t], send, recv, peer)]
+
+    for copy in spread(acts_mine, acts_in, act_sem.at[0], act_sem.at[1], 2):
+        copy.start()
+
     conv_read = conv[:, width + STATE :]
-    inner = lax.dot_general(
-        conv_read, conv_write, (((1,), (1,)), ((), ())), preferred_element_type=F32
-    )
-    causal = row_id >= col_id
-    for j in range(pairs):
-        tile = conv[:, j * LANES : (j + 1) * LANES]
-        parts = []
-        for h in (2 * j, 2 * j + 1):
-            gap = jnp.where(causal, cum_col[:, h : h + 1] - cum[h : h + 1, :], NEGATIVE)
-            weights = (inner * (jnp.exp(gap) * step[h : h + 1, :])).astype(BF16)
-            parts.append(jnp.dot(weights, tile, preferred_element_type=F32))
-        bypass = jnp.where(low, bypass_ref[2 * j], bypass_ref[2 * j + 1])
-        mix[:, j * LANES : (j + 1) * LANES] = (
-            jnp.where(low, parts[0], parts[1]) + bypass * tile.astype(F32)
-        )
-
     squares = []
     for p in range(pairs):
         at = slice(p * LANES, (p + 1) * LANES)
 
-        @pl.when(jnp.logical_and(me > 0, jnp.logical_not(relays)))
+        @pl.when(me == sp - 1)
         def _(p=p):
-            state_copy(p, 1).wait_recv()
-            entered(p)
+            state_copy(p).wait_recv()
 
         carried = jnp.dot(conv_read, state_in[p], preferred_element_type=F32)
         gate = gate_ref[0, :, at].astype(F32)
@@ -731,10 +666,10 @@
         squares.append(u * u)
         sent = (u * gain_ref[0:1, at]).astype(BF16)
         for r in range(2):
-            pieces_mine[r, p] = sent[r * half : (r + 1) * half]
-        for slot in slots:
-            for copy in piece_copies(p, slot):
-                copy.start()
+            pieces_mine[p, r] = sent[r * half : (r + 1) * half]
+        recv = piece_recv.at[0 if p < pairs - 1 else 1]
+        for copy in spread(pieces_mine.at[p], pieces_in.at[p], piece_send.at[0], recv, 1):
+            copy.start()
 
     total = functools.reduce(jnp.add, squares)
     mean = (
@@ -750,152 +685,111 @@
     scale = lax.rsqrt(mean + EPSILON)
     scales_mine[0] = scale
     scales_mine[1] = pltpu.roll(scale, half, 1)
-    for slot in slots:
-        for copy in piece_copies(pairs, slot):
-            copy.start()
-
-    acts_in[0, t] = acts_mine[t]
+    for copy in spread(scales_mine, scales_in, piece_send.at[1], piece_recv.at[2], 1):
+        copy.start()
+
+    acts_in[t] = acts_mine[t]
     for p in range(pairs):
-        pieces_in[0, t, p] = pieces_mine[t, p]
-    scales_in[0, t] = scales_mine[t]
-
-    for i in (1, 0):
-        for kind in (1, 2):
-            weight_copy(kind, i).wait_recv()
-            weight_copy(kind + 2, i).start()
-
-    groups = (
-        (2, wst, wat, first),
-        (2, wst_x, wat_x, slice(0, part)),
-        (1, wst, wat, second),
-        (1, wst_y, wat_y, slice(0, part)),
-    )
-    needs = (0, 3, 0, 4)
-
-    def from_peer(kind, i):
-        whole, from_x, from_y = matrices[i]
-        ref = (whole, None, None, from_x, from_y)[kind]
-        remote(
-            ref.at[1 - t],
-            ref.at[1 - t],
-            weight_send.at[kind, i],
-            weight_recv.at[kind, i],
-            {"tp": 1 - t},
-        ).wait_recv()
-
-    act_wait(0, 1 - t)
-    for slot in (2, 1):
-        for source in range(2):
-            act_wait(slot, source)
-    for kind in (0, 3, 4):
-        from_peer(kind, 1)
-    for g, (slot, _, weights, at) in enumerate(groups):
+        pieces_in[p, t] = pieces_mine[p, t]
+    scales_in[t] = scales_mine[t]
+
+    for i, ref in enumerate((wat_x, wst_y)):
+        arrived(ref.at[t], weight_recv.at[i])
+        weight_copies(2)[i].start()
+
+    def groups(own, other):
+        return [(ref, slice(h * part, (h + 1) * part)) for ref in (own, other) for h in range(2)]
+
+    def back(out, landing, g, send, recv, hop):
+        return remote(out.at[g], landing.at[g], send, recv, {"fs": f ^ hop})
+
+    arrived(acts_in.at[0:3], act_sem.at[1])
+    arrived(wat, weight_recv.at[2])
+    left = jnp.concatenate(
+        [jnp.concatenate([acts_in[s], acts_in[2 + s]], axis=0) for s in range(2)], axis=1
+    )
+    for g, (weights, at) in enumerate(groups(wat, wat_x)):
+        right = jnp.concatenate([weights[s, :, at] for s in range(2)], axis=0)
+        product = jnp.dot(left, right, preferred_element_type=F32)
+        acc[g] = product[0:half]
+        att_out[g] = product[half:].astype(BF16)
+        back(att_out, att_in, g, sum_send.at[0], sum_recv.at[0], 2).start()
+
+    arrived(wst, weight_recv.at[3])
+    arrived(pieces_in.at[0 : pairs - 1, 0:3], piece_recv.at[0])
+    cut = (pairs - 1) * LANES
+    for s in range(2):
         left = jnp.concatenate(
             [
-                jnp.concatenate([acts_in[0, s], acts_in[slot, s]], axis=0)
-                for s in range(2)
+                jnp.concatenate([pieces_in[p, s], pieces_in[p, 2 + s]], axis=0)
+                for p in range(pairs - 1)
             ],
             axis=1,
         )
-        right = jnp.concatenate([weights[s, :, at] for s in range(2)], axis=0)
-        acc[g] = jnp.dot(left, right, preferred_element_type=F32)
-
-    for kind in (0, 3, 4):
-        from_peer(kind, 0)
-    for p in range(pairs - 1):
-        piece_wait(p, 0, 1 - t)
-        for slot in (2, 1):
-            for source in range(2):
-                piece_wait(p, slot, source)
-
-    cut = (pairs - 1) * LANES
-
-    def stacked(slot, s, p):
-        return jnp.concatenate([pieces_in[0, s, p], pieces_in[slot, s, p]], axis=0)
-
-    for g, (slot, weights, _, at) in enumerate(groups):
-        for s in range(2):
-            left = jnp.concatenate([stacked(slot, s, p) for p in range(pairs - 1)], axis=1)
+        for g, (weights, at) in enumerate(groups(wst, wst_y)):
             acc_state[g, s] = jnp.dot(left, weights[s, 0:cut, at], preferred_element_type=F32)
 
-    for p in (pairs - 1, pairs):
-        piece_wait(p, 0, 1 - t)
-        for slot in (2, 1):
-            for source in range(2):
-                piece_wait(p, slot, source)
-
-    def columns(owner, at):
-        return pl.ds(pl.multiple_of(owner * cols + at.start, part), part)
-
-    def sum_copy(g):
-        slot = groups[g][0]
-        owner = (f, f ^ 1, f, f ^ 2)[g]
-        at = (first, first, second, second)[g]
-        return remote(
-            returned.at[g],
-            out_ref.at[0, :, columns(owner, at)],
-            sum_send.at[g],
-            sum_recv.at[g],
-            {"fs": f ^ slot},
+    arrived(pieces_in.at[pairs - 1, 0:3], piece_recv.at[1])
+    arrived(scales_in.at[0:3], piece_recv.at[2])
+    by = [scales_in[i].T[0:half, 0:1] for i in range(4)]
+
+    def state_sum(g, weights, at, slot):
+        here = slice(slot // 2 * half, (slot // 2 + 1) * half)
+        return functools.reduce(
+            jnp.add,
+            [
+                (
+                    acc_state[g, s, here]
+                    + jnp.dot(
+                        pieces_in[pairs - 1, slot + s],
+                        weights[s, cut:, at],
+                        preferred_element_type=F32,
+                    )
+                )
+                * by[slot + s]
+                for s in range(2)
+            ],
         )
 
-    turned = [[scales_in[slot, s].T[0:half, 0:1] for s in range(2)] for slot in range(3)]
-    for g, (slot, weights, _, at) in enumerate(groups):
-        merged = acc[g]
-        for s in range(2):
-            last = jnp.dot(
-                stacked(slot, s, pairs - 1), weights[s, cut:, at], preferred_element_type=F32
-            )
-            by = jnp.concatenate([turned[0][s], turned[slot][s]], axis=0)
-            merged = merged + (acc_state[g, s] + last) * by
-        merged = merged.astype(BF16)
-        returned[g] = merged[half:]
-        sum_copy(g).start()
-        owner = (f, f ^ 1, f, f ^ 2)[g]
-        out_ref[0, :, columns(owner, (first, first, second, second)[g])] = merged[0:half]
-
-    for g in range(4):
-        sum_copy(g).wait_recv()
+    for g, (weights, at) in enumerate(groups(wst, wst_y)):
+        sum_out[g] = state_sum(g, weights, at, 2).astype(BF16)
+        back(sum_out, sum_in, g, sum_send.at[1], sum_recv.at[1], 1).start()
+
+    def place(owner, h, values):
+        at = pl.ds(pl.multiple_of(owner * cols + h * part, part), part)
+        out_ref[0, :, at] = values.astype(BF16)
+
+    arrived(att_in, sum_recv.at[0])
+    for g, (weights, at) in enumerate(groups(wst, wst_y)):
+        mine = state_sum(g, weights, at, 0)
+        if g < 2:
+            place(f, g, acc[g] + mine)
+        else:
+            place(f ^ 2, g - 2, att_in[g - 2].astype(F32) + mine)
+    arrived(sum_in, sum_recv.at[1])
+    for h in range(2):
+        place(f ^ 1, h, acc[2 + h] + sum_in[h].astype(F32))
+        place(f ^ 3, h, att_in[2 + h].astype(F32) + sum_in[2 + h].astype(F32))
 
     @pl.when(follows)
     def _():
-        for copy in tail:
-            copy.wait_send()
-
-    @pl.when(jnp.logical_and(follows, jnp.logical_or(odd, me == 0)))
-    def _():
-        for p in range(pairs):
-            state_copy(p, 1).wait_send()
-
-    @pl.when(jnp.logical_and(odd, me + 2 < sp))
-    def _():
-        for p in range(pairs):
-            state_copy(p, 2).wait_send()
-
-    @pl.when(jnp.logical_and(jnp.logical_not(odd), jnp.logical_and(me > 0, follows)))
-    def _():
-        for p in range(pairs):
-            side_copy(p).wait_send()
-        side_decay_copy().wait_send()
-
-    for d in range(1, sp):
-
-        @pl.when(me + d < sp)
-        def _(d=d):
-            for copy in kv_copies(d, me):
-                copy.wait_send()
-
-    for kind in range(5):
-        for i in range(2):
-            weight_copy(kind, i).wait_send()
-    for slot in slots:
-        for copy in act_copies(slot):
-            copy.wait_send()
-        for p in range(pairs + 1):
-            for copy in piece_copies(p, slot):
-                copy.wait_send()
-    for g in range(4):
-        sum_copy(g).wait_send()
+        departed(tails, tail_sem.at[0])
+        departed(state_out, st_send)
+
+    for n in range(1, sp):
+
+        @pl.when(sp - 1 - me == n)
+        def _(n=n):
+            departed(kvall.at[0:n], kv_sem.at[0])
+            departed(gall.at[0:n], kv_sem.at[2])
+
+    for kind in range(3):
+        departed(wst, weight_send.at[kind])
+    departed(acts_in.at[0:3], act_sem.at[0])
+    departed(pieces_in.at[:, 0:3], piece_send.at[0])
+    departed(scales_in.at[0:3], piece_send.at[1])
+    departed(att_out, sum_send.at[0])
+    departed(sum_out, sum_send.at[1])
 
 
 def fused(sp, fs, *args):
@@ -906,7 +800,6 @@
     args = list(args)
     args[11] = args[11].reshape(1, -1)
     args[15] = jnp.swapaxes(args[15], 1, 2)
-    vmem = pl.BlockSpec(memory_space=pltpu.VMEM)
     far = pl.BlockSpec(memory_space=pl.ANY)
     dma = pltpu.SemaphoreType.DMA
     kv_width = args[13].shape[2]
@@ -915,60 +808,55 @@
     near = [
         (pltpu.SMEM if i in (6, 7) else pltpu.VMEM)(a.shape, a.dtype)
         for i, a in enumerate(args[:16])
+        if i not in (13, 14)
     ]
     return pl.pallas_call(
         functools.partial(mixer_kernel, sp, fs),
-        out_shape=jax.ShapeDtypeStruct((1, half, cols * fs), BF16),
+        out_shape=pltpu.VMEM((1, half, cols * fs), BF16),
         in_specs=[far] * len(args),
-        out_specs=vmem,
+        out_specs=pl.BlockSpec(memory_space=pltpu.VMEM),
         scratch_shapes=near
         + [
             dma((len(args),)),
+            pltpu.SemaphoreType.REGULAR((sp - 1,)),
             pltpu.VMEM((8 + rows, width + 2 * STATE), F32),
             pltpu.VMEM((16, width + 2 * STATE), BF16),
             pltpu.VMEM((rows, width + 2 * STATE), BF16),
             pltpu.VMEM((rows, width), F32),
-            pltpu.VMEM((sp, rows, kv_width), BF16),
-            pltpu.VMEM((sp, rows, kv_width), BF16),
+            pltpu.VMEM((sp, rows, 2 * kv_width), BF16),
             pltpu.VMEM((sp, heads, rows), F32),
             pltpu.VMEM((kv_heads, heads // kv_heads * rows, kv_width), BF16),
             pltpu.VMEM((pairs, STATE, LANES), F32),
             pltpu.VMEM((pairs, STATE, LANES), BF16),
             pltpu.VMEM((pairs, STATE, LANES), BF16),
-            pltpu.VMEM((pairs, STATE, LANES), BF16),
-            pltpu.VMEM((heads, LANES), F32),
-            pltpu.VMEM((heads, LANES), F32),
             pltpu.VMEM((rows, width), F32),
             pltpu.VMEM((2, deep, cols), BF16),
             pltpu.VMEM((2, deep, cols), BF16),
-            pltpu.VMEM((2, deep, part), BF16),
-            pltpu.VMEM((2, deep, part), BF16),
-            pltpu.VMEM((2, deep, part), BF16),
-            pltpu.VMEM((2, deep, part), BF16),
+            pltpu.VMEM((2, deep, cols), BF16),
+            pltpu.VMEM((2, deep, cols), BF16),
             pltpu.VMEM((2, half, width), BF16),
-            pltpu.VMEM((3, 2, half, width), BF16),
-            pltpu.VMEM((2, pairs, half, LANES), BF16),
-            pltpu.VMEM((3, 2, pairs, half, LANES), BF16),
+            pltpu.VMEM((4, half, width), BF16),
+            pltpu.VMEM((pairs, 2, half, LANES), BF16),
+            pltpu.VMEM((pairs, 4, half, LANES), BF16),
             pltpu.VMEM((2, 8, rows), F32),
-            pltpu.VMEM((3, 2, 8, rows), F32),
-            pltpu.VMEM((4, rows, part), F32),
+            pltpu.VMEM((4, 8, rows), F32),
+            pltpu.VMEM((4, half, part), F32),
             pltpu.VMEM((4, 2, rows, part), F32),
             pltpu.VMEM((4, half, part), BF16),
+            pltpu.VMEM((4, half, part), BF16),
+            pltpu.VMEM((4, half, part), BF16),
+            pltpu.VMEM((4, half, part), BF16),
+            dma((2,)),
+            dma((4,)),
+            dma,
+            dma((pairs,)),
             dma((3,)),
+            dma((4,)),
+            dma((2,)),
+            dma((2,)),
             dma((3,)),
-            dma((sp, 3)),
-            dma((sp, 3)),
-            dma((pairs + 1, 2)),
-            dma((pairs,)),
-            dma((pairs + 1,)),
-            dma((5, 2)),
-            dma((5, 2)),
-            dma((3, 2)),
-            dma((3, 2)),
-            dma((pairs + 1, 3, 2)),
-            dma((pairs + 1, 3, 2)),
-            dma((4,)),
-            dma((4,)),
+            dma((2,)),
+            dma((2,)),
         ],
         compiler_params=pltpu.CompilerParams(collective_id=0, has_side_effects=True),
     )(*args)

time: 32.5 us -> 27.4 us (0.84)
  the two profiles are of different devices: /device:TPU:0 before, /device:TPU:17 now
where the time goes in v2:
time: 27.4 us; the launch traced here: 27.3 us
  Pallas kernels  26.5 us (97%)
  local copies, waits for them, and re-layouts  0.71 us (3%)
    pallas_call x1, Pallas kernels, fused(): pl.pallas_call(functools.partial(mixer_kernel, sp, fs), out_shape=pltpu.V...  26.5 us
    unnamed x1, local copies, waits for them, and re-layouts  0.71 us

profile of v2, /device:TPU:17, one launch (start us, length us, event | category | flops | bytes accessed | tf_op | source)
XLA Modules:
  0.0 27.3 jit_solution(12533746093474454137)
XLA Ops:
  0.0 26.5 %shard_map.172 = bf16[1,64,2048]{2,1,0:T(8,128)(2,1)S(1)} custom-call(bf16[1,128,512]{2,1,0:T(8,128)(2,1)} %x_far.1, bf16[1,128,128]{2,1,0:T(8,128)(2,1)} %w_far.1, bf16[1,128,128]{2,1,0:T(8,128)(2,1)} %r_far.1, bf16[1,128,512]{2,1,0:T(8,128)(2,1)} %gate_far.1, f32[1,8,128]{2,1,0:T(8,128)} %step_far.1, f32[1,8,128]{2,1,0:T(8,128)} %extra_far.1, ...), custom_call_target="tpu_custom_call" | custom-call | tf_op jit(solution)/shard_map/pallas_call | solution.py:813
  26.5 0.7 %copy.20 = bf16[1,64,2048]{2,1,0:T(8,128)(2,1)} copy(bf16[1,64,2048]{2,1,0:T(8,128)(2,1)S(1)} %shard_map.172) | data formatting | bytes 524288

commit v3 on v2

--- a/solution.py
+++ b/solution.py
@@ -349,6 +349,10 @@
         def _(d=d):
             pl.semaphore_signal(barrier, inc=1, device_id={"sp": me + d}, device_id_type=MESH)
 
+    @pl.when(me > 0)
+    def _():
+        pl.semaphore_signal(barrier, inc=1, device_id={"sp": me - 1}, device_id_type=MESH)
+
     near = {
         "x": (x_far, x_ref),
         "w": (w_far, w_ref),
@@ -396,36 +400,16 @@
     def departed(ref, sem):
         remote(ref, ref, sem, sem, peer).wait_send()
 
-    lane = lax.broadcasted_iota(jnp.int32, (1, LANES), 1)
-    low = lane < HEAD_DIM
-    row_id = lax.broadcasted_iota(jnp.int32, (rows, rows), 0)
-    col_id = lax.broadcasted_iota(jnp.int32, (rows, rows), 1)
-
-    def expand(columns, j):
-        return jnp.where(low, columns[:, 2 * j : 2 * j + 1], columns[:, 2 * j + 1 : 2 * j + 2])
-
-    inputs = (
-        (x_ref, tapx_ref, slice(0, width)),
-        (w_ref, tapw_ref, slice(width, width + STATE)),
-        (r_ref, tapr_ref, slice(width + STATE, width + 2 * STATE)),
-    )
-
-    def filtered(count):
-        for _, tap_ref, at in inputs:
-            total = jnp.zeros((count, at.stop - at.start), F32)
-            for i in range(taps):
-                first = 8 - (taps - 1) + i
-                total = total + tap_ref[i : i + 1, :].astype(F32) * pad_ref[first : first + count, at]
-            conv[0:count, at] = (total * jax.nn.sigmoid(total)).astype(BF16)
-
-    pad_ref[0:8, :] = jnp.zeros((8, pad_ref.shape[1]), F32)
-    loaded("x", "w", "r", "tapx", "tapw", "tapr")
-    for ref, _, at in inputs:
-        pad_ref[8 : 8 + rows, at] = ref[0].astype(F32)
-    filtered(rows)
-
-    loaded("wat", "wst")
-    pl.semaphore_wait(barrier, 5 + me)
+    follows = me + 1 < sp
+    pl.semaphore_wait(barrier, 5 + me + jnp.where(follows, 1, 0))
+
+    for d in range(2, sp):
+
+        @pl.when(me - d >= 0)
+        def _(d=d):
+            pl.semaphore_signal(
+                ready.at[d - 2], inc=1, device_id={"sp": me - d}, device_id_type=MESH
+            )
 
     def weight_copies(kind):
         return (
@@ -443,17 +427,38 @@
             ),
         )[kind]
 
+    loaded("wat", "wst")
     for kind in range(2):
         for copy in weight_copies(kind):
             copy.start()
 
-    for d in range(1, sp):
-
-        @pl.when(me - d >= 0)
-        def _(d=d):
-            pl.semaphore_signal(
-                ready.at[d - 1], inc=1, device_id={"sp": me - d}, device_id_type=MESH
-            )
+    lane = lax.broadcasted_iota(jnp.int32, (1, LANES), 1)
+    low = lane < HEAD_DIM
+    row_id = lax.broadcasted_iota(jnp.int32, (rows, rows), 0)
+    col_id = lax.broadcasted_iota(jnp.int32, (rows, rows), 1)
+
+    def expand(columns, j):
+        return jnp.where(low, columns[:, 2 * j : 2 * j + 1], columns[:, 2 * j + 1 : 2 * j + 2])
+
+    inputs = (
+        (x_ref, tapx_ref, slice(0, width)),
+        (w_ref, tapw_ref, slice(width, width + STATE)),
+        (r_ref, tapr_ref, slice(width + STATE, width + 2 * STATE)),
+    )
+
+    def filtered(count):
+        for _, tap_ref, at in inputs:
+            total = jnp.zeros((count, at.stop - at.start), F32)
+            for i in range(taps):
+                first = 8 - (taps - 1) + i
+                total = total + tap_ref[i : i + 1, :].astype(F32) * pad_ref[first : first + count, at]
+            conv[0:count, at] = (total * jax.nn.sigmoid(total)).astype(BF16)
+
+    pad_ref[0:8, :] = jnp.zeros((8, pad_ref.shape[1]), F32)
+    loaded("x", "w", "r", "tapx", "tapw", "tapr")
+    for ref, _, at in inputs:
+        pad_ref[8 : 8 + rows, at] = ref[0].astype(F32)
+    filtered(rows)
 
     loaded("step", "extra", "shrink")
     head_row = lax.broadcasted_iota(jnp.int32, (heads, rows), 0)
@@ -472,8 +477,6 @@
     for j in range(pairs):
         end_wide[:, j * LANES : (j + 1) * LANES] = expand(end_scale, j)
 
-    follows = me + 1 < sp
-
     def own_states():
         turned_write = conv[:, width : width + STATE].astype(F32).T.astype(BF16)
         for p in range(pairs):
@@ -516,7 +519,6 @@
 
     @pl.when(follows)
     def _():
-        pl.semaphore_wait(ready.at[0], 1)
         for copy in tail:
             copy.start()
 
@@ -530,7 +532,7 @@
         @pl.when(me + d < sp)
         def _(d=d):
             if d > 1:
-                pl.semaphore_wait(ready.at[d - 1], 1)
+                pl.semaphore_wait(ready.at[d - 2], 1)
             for copy in kv_copies(d):
                 copy.start()
 
@@ -585,15 +587,16 @@
     def _():
         within()
 
-    relays = jnp.logical_and(me > 0, follows)
-
-    @pl.when(relays)
-    def _():
+    def relay():
         for p in range(pairs):
             state_copy(p).wait_recv()
             decay = jnp.where(low, decays[2 * p : 2 * p + 1, :], decays[2 * p + 1 : 2 * p + 2, :])
             state_out[p] = (state_in[p].astype(F32) * decay + own_state[p]).astype(BF16)
             state_copy(p).start()
+
+    @pl.when(jnp.logical_and(me == 1, follows))
+    def _():
+        relay()
 
     @pl.when(me == 1)
     def _():
@@ -651,6 +654,10 @@
     for copy in spread(acts_mine, acts_in, act_sem.at[0], act_sem.at[1], 2):
         copy.start()
 
+    @pl.when(jnp.logical_and(me > 1, follows))
+    def _():
+        relay()
+
     conv_read = conv[:, width + STATE :]
     squares = []
     for p in range(pairs):
@@ -672,12 +679,13 @@
             copy.start()
 
     total = functools.reduce(jnp.add, squares)
+    coarse = total.astype(BF16)
+    fine = (total - coarse.astype(F32)).astype(BF16)
     mean = (
         lax.dot_general(
-            jnp.ones((8, LANES), F32),
-            total,
+            jnp.ones((8, 2 * LANES), BF16),
+            jnp.concatenate([coarse, fine], axis=1),
             (((1,), (1,)), ((), ())),
-            precision=lax.Precision.HIGHEST,
             preferred_element_type=F32,
         )
         / width
@@ -708,12 +716,14 @@
     left = jnp.concatenate(
         [jnp.concatenate([acts_in[s], acts_in[2 + s]], axis=0) for s in range(2)], axis=1
     )
-    for g, (weights, at) in enumerate(groups(wat, wat_x)):
-        right = jnp.concatenate([weights[s, :, at] for s in range(2)], axis=0)
-        product = jnp.dot(left, right, preferred_element_type=F32)
-        acc[g] = product[0:half]
-        att_out[g] = product[half:].astype(BF16)
-        back(att_out, att_in, g, sum_send.at[0], sum_recv.at[0], 2).start()
+    for pair in (0, 2):
+        for g, (weights, at) in list(enumerate(groups(wat, wat_x)))[pair : pair + 2]:
+            right = jnp.concatenate([weights[s, :, at] for s in range(2)], axis=0)
+            product = jnp.dot(left, right, preferred_element_type=F32)
+            acc[g] = product[0:half]
+            att_out[g] = product[half:].astype(BF16)
+        for g in (pair, pair + 1):
+            back(att_out, att_in, g, sum_send.at[0], sum_recv.at[0], 2).start()
 
     arrived(wst, weight_recv.at[3])
     arrived(pieces_in.at[0 : pairs - 1, 0:3], piece_recv.at[0])
@@ -731,7 +741,8 @@
 
     arrived(pieces_in.at[pairs - 1, 0:3], piece_recv.at[1])
     arrived(scales_in.at[0:3], piece_recv.at[2])
-    by = [scales_in[i].T[0:half, 0:1] for i in range(4)]
+    upright = scales_in[...].reshape(4 * 8, rows).T
+    by = [upright[0:half, 8 * i : 8 * i + 1] for i in range(4)]
 
     def state_sum(g, weights, at, slot):
         here = slice(slot // 2 * half, (slot // 2 + 1) * half)
@@ -751,9 +762,11 @@
             ],
         )
 
-    for g, (weights, at) in enumerate(groups(wst, wst_y)):
-        sum_out[g] = state_sum(g, weights, at, 2).astype(BF16)
-        back(sum_out, sum_in, g, sum_send.at[1], sum_recv.at[1], 1).start()
+    for pair in (0, 2):
+        for g, (weights, at) in list(enumerate(groups(wst, wst_y)))[pair : pair + 2]:
+            sum_out[g] = state_sum(g, weights, at, 2).astype(BF16)
+        for g in (pair, pair + 1):
+            back(sum_out, sum_in, g, sum_send.at[1], sum_recv.at[1], 1).start()
 
     def place(owner, h, values):
         at = pl.ds(pl.multiple_of(owner * cols + h * part, part), part)
@@ -818,7 +831,7 @@
         scratch_shapes=near
         + [
             dma((len(args),)),
-            pltpu.SemaphoreType.REGULAR((sp - 1,)),
+            pltpu.SemaphoreType.REGULAR((max(sp - 2, 1),)),
             pltpu.VMEM((8 + rows, width + 2 * STATE), F32),
             pltpu.VMEM((16, width + 2 * STATE), BF16),
             pltpu.VMEM((rows, width + 2 * STATE), BF16),

time: 27.4 us -> 26.6 us (0.971)
  the two profiles are of different devices: /device:TPU:17 before, /device:TPU:24 now
where the time goes in v3:
time: 26.6 us; the launch traced here: 26 us
  Pallas kernels  25.3 us (95%)
  local copies, waits for them, and re-layouts  0.71 us (3%)
    pallas_call x1, Pallas kernels, fused(): pl.pallas_call(functools.partial(mixer_kernel, sp, fs), out_shape=pltpu.V...  25.3 us
    unnamed x1, local copies, waits for them, and re-layouts  0.71 us

profile of v3, /device:TPU:24, one launch (start us, length us, event | category | flops | bytes accessed | tf_op | source)
XLA Modules:
  0.0 26.0 jit_solution(11156351699986655269)
XLA Ops:
  0.0 25.3 %shard_map.172 = bf16[1,64,2048]{2,1,0:T(8,128)(2,1)S(1)} custom-call(bf16[1,128,512]{2,1,0:T(8,128)(2,1)} %x_far.1, bf16[1,128,128]{2,1,0:T(8,128)(2,1)} %w_far.1, bf16[1,128,128]{2,1,0:T(8,128)(2,1)} %r_far.1, bf16[1,128,512]{2,1,0:T(8,128)(2,1)} %gate_far.1, f32[1,8,128]{2,1,0:T(8,128)} %step_far.1, f32[1,8,128]{2,1,0:T(8,128)} %extra_far.1, ...), custom_call_target="tpu_custom_call" | custom-call | tf_op jit(solution)/shard_map/pallas_call | solution.py:826
  25.3 0.7 %copy.20 = bf16[1,64,2048]{2,1,0:T(8,128)(2,1)} copy(bf16[1,64,2048]{2,1,0:T(8,128)(2,1)S(1)} %shard_map.172) | data formatting | bytes 524288

commit v4 on v3

--- a/solution.py
+++ b/solution.py
@@ -285,6 +285,7 @@
     pad_ref,
     tails,
     conv,
+    soft_cum,
     end_wide,
     kvall,
     gall,
@@ -304,7 +305,6 @@
     scales_mine,
     scales_in,
     acc,
-    acc_state,
     att_out,
     att_in,
     sum_out,
@@ -315,9 +315,12 @@
     st_recv,
     weight_send,
     weight_recv,
-    act_sem,
+    peer_recv,
+    act_send,
+    act_recv,
     piece_send,
     piece_recv,
+    scale_recv,
     sum_send,
     sum_recv,
 ):
@@ -400,38 +403,6 @@
     def departed(ref, sem):
         remote(ref, ref, sem, sem, peer).wait_send()
 
-    follows = me + 1 < sp
-    pl.semaphore_wait(barrier, 5 + me + jnp.where(follows, 1, 0))
-
-    for d in range(2, sp):
-
-        @pl.when(me - d >= 0)
-        def _(d=d):
-            pl.semaphore_signal(
-                ready.at[d - 2], inc=1, device_id={"sp": me - d}, device_id_type=MESH
-            )
-
-    def weight_copies(kind):
-        return (
-            (
-                remote(wat.at[t], wat_x.at[t], weight_send.at[0], weight_recv.at[0], {"fs": f ^ 1}),
-                remote(wst.at[t], wst_y.at[t], weight_send.at[0], weight_recv.at[1], {"fs": f ^ 2}),
-            ),
-            (
-                remote(wat.at[t], wat.at[t], weight_send.at[1], weight_recv.at[2], peer),
-                remote(wst.at[t], wst.at[t], weight_send.at[1], weight_recv.at[3], peer),
-            ),
-            (
-                remote(wat_x.at[t], wat_x.at[t], weight_send.at[2], weight_recv.at[2], peer),
-                remote(wst_y.at[t], wst_y.at[t], weight_send.at[2], weight_recv.at[3], peer),
-            ),
-        )[kind]
-
-    loaded("wat", "wst")
-    for kind in range(2):
-        for copy in weight_copies(kind):
-            copy.start()
-
     lane = lax.broadcasted_iota(jnp.int32, (1, LANES), 1)
     low = lane < HEAD_DIM
     row_id = lax.broadcasted_iota(jnp.int32, (rows, rows), 0)
@@ -460,22 +431,22 @@
         pad_ref[8 : 8 + rows, at] = ref[0].astype(F32)
     filtered(rows)
 
-    loaded("step", "extra", "shrink")
-    head_row = lax.broadcasted_iota(jnp.int32, (heads, rows), 0)
-    power = jnp.zeros((heads, rows), F32)
-    for h in range(heads):
-        power = jnp.where(head_row == h, shrink_ref[h], power)
-    presoft = step_ref[0]
-    step = jnp.maximum(presoft, 0.0) + jnp.log1p(jnp.exp(-jnp.abs(presoft)))
-    log_decay = extra_ref[0] - jnp.exp(power) * step
-    upper = (row_id <= col_id).astype(F32)
-    cum = jnp.dot(log_decay, upper, precision=lax.Precision.HIGHEST, preferred_element_type=F32)
-    cum_end = cum[:, rows - 1 : rows]
-    decays = jnp.broadcast_to(jnp.exp(cum_end), (heads, LANES))
-
-    end_scale = (jnp.exp(cum_end - cum) * step).T
-    for j in range(pairs):
-        end_wide[:, j * LANES : (j + 1) * LANES] = expand(end_scale, j)
+    def decay():
+        loaded("step", "extra", "shrink")
+        head_row = lax.broadcasted_iota(jnp.int32, (heads, rows), 0)
+        power = jnp.zeros((heads, rows), F32)
+        for h in range(heads):
+            power = jnp.where(head_row == h, shrink_ref[h], power)
+        presoft = step_ref[0]
+        step = jnp.maximum(presoft, 0.0) + jnp.log1p(jnp.exp(-jnp.abs(presoft)))
+        log_decay = extra_ref[0] - jnp.exp(power) * step
+        upper = (row_id <= col_id).astype(F32)
+        cum = jnp.dot(log_decay, upper, precision=lax.Precision.HIGHEST, preferred_element_type=F32)
+        soft_cum[0] = step
+        soft_cum[1] = cum
+        end_scale = (jnp.exp(cum[:, rows - 1 : rows] - cum) * step).T
+        for j in range(pairs):
+            end_wide[:, j * LANES : (j + 1) * LANES] = expand(end_scale, j)
 
     def own_states():
         turned_write = conv[:, width : width + STATE].astype(F32).T.astype(BF16)
@@ -484,16 +455,63 @@
             weighted = (conv[:, at].astype(F32) * end_wide[:, at]).astype(BF16)
             own_state[p] = jnp.dot(turned_write, weighted, preferred_element_type=F32)
 
+    @pl.when(me == 0)
+    def _():
+        state_in[...] = jnp.zeros(state_in.shape, BF16)
+        decay()
+        own_states()
+        for p in range(pairs):
+            state_out[p] = own_state[p].astype(BF16)
+
+    follows = me + 1 < sp
+    pl.semaphore_wait(barrier, 5 + me + jnp.where(follows, 1, 0))
+
+    for d in range(2, sp):
+
+        @pl.when(me - d >= 0)
+        def _(d=d):
+            pl.semaphore_signal(
+                ready.at[d - 2], inc=1, device_id={"sp": me - d}, device_id_type=MESH
+            )
+
+    deep = wst_far.shape[0]
+    chunks = (slice(0, deep * 3 // 4), slice(deep * 3 // 4, deep))
+
+    def weight_copies(chunk):
+        at = (t, chunks[chunk])
+        return [
+            remote(
+                src.at[at], dst.at[at], weight_send.at[0], weight_recv.at[i, chunk], {"fs": f ^ hop}
+            )
+            for i, (src, dst, hop) in enumerate(((wat, wat_x, 1), (wst, wst_y, 2)))
+        ]
+
+    def own_copies():
+        return [
+            remote(w.at[t], w.at[t], weight_send.at[1], peer_recv.at[0], peer) for w in (wat, wst)
+        ]
+
+    def relay_copies(chunk):
+        at = (t, chunks[chunk])
+        return [
+            remote(w.at[at], w.at[at], weight_send.at[2], peer_recv.at[1], peer)
+            for w in (wat_x, wst_y)
+        ]
+
+    loaded("wat", "wst")
+    for copy in weight_copies(0) + weight_copies(1) + own_copies():
+        copy.start()
+
+    @pl.when(me > 0)
+    def _():
+        decay()
+
+    step, cum = soft_cum[0], soft_cum[1]
+    decays = jnp.broadcast_to(jnp.exp(cum[:, rows - 1 : rows]), (heads, LANES))
+
     def state_copy(p):
         there = {"sp": lax.rem(me + 1, sp)}
         return remote(state_out.at[p], state_in.at[p], st_send, st_recv.at[p], there)
-
-    @pl.when(me == 0)
-    def _():
-        state_in[...] = jnp.zeros(state_in.shape, BF16)
-        own_states()
-        for p in range(pairs):
-            state_out[p] = own_state[p].astype(BF16)
 
     loaded("k", "v", "forget")
     gall[me] = forget_ref[0]
@@ -527,14 +545,21 @@
         for p in range(pairs):
             state_copy(p).start()
 
-    for d in range(1, sp):
-
-        @pl.when(me + d < sp)
-        def _(d=d):
-            if d > 1:
+    @pl.when(follows)
+    def _():
+        for copy in kv_copies(1):
+            copy.start()
+
+    def far_kv(fits):
+        for d in range(2, sp):
+
+            @pl.when(jnp.logical_and(fits, me + d < sp))
+            def _(d=d):
                 pl.semaphore_wait(ready.at[d - 2], 1)
-            for copy in kv_copies(d):
-                copy.start()
+                for copy in kv_copies(d):
+                    copy.start()
+
+    far_kv(me > 0)
 
     for j in range(1, sp):
 
@@ -645,14 +670,28 @@
             for r in range(2):
                 acts_mine[r, :, at] = merged[r * half : (r + 1) * half]
 
-    def spread(src, dst, send, recv, hop):
+    quarter = half // 2
+    spans = (slice(0, quarter), slice(quarter, half))
+
+    def spread(src, dst, send, recv, hop, q):
         return [
-            remote(src.at[r], dst.at[2 + t], send, recv, {"fs": f ^ hop, "tp": r})
+            remote(
+                src.at[r, spans[q]],
+                dst.at[2 + t, spans[q]],
+                send,
+                recv.at[1 + q],
+                {"fs": f ^ hop, "tp": r},
+            )
             for r in range(2)
-        ] + [remote(src.at[1 - t], dst.at[t], send, recv, peer)]
-
-    for copy in spread(acts_mine, acts_in, act_sem.at[0], act_sem.at[1], 2):
-        copy.start()
+        ]
+
+    def across(src, dst, send, recv):
+        return remote(src.at[1 - t], dst.at[t], send, recv.at[0], peer)
+
+    for q in range(2):
+        for copy in spread(acts_mine, acts_in, act_send, act_recv, 2, q):
+            copy.start()
+    across(acts_mine, acts_in, act_send, act_recv).start()
 
     @pl.when(jnp.logical_and(me > 1, follows))
     def _():
@@ -674,9 +713,9 @@
         sent = (u * gain_ref[0:1, at]).astype(BF16)
         for r in range(2):
             pieces_mine[p, r] = sent[r * half : (r + 1) * half]
-        recv = piece_recv.at[0 if p < pairs - 1 else 1]
-        for copy in spread(pieces_mine.at[p], pieces_in.at[p], piece_send.at[0], recv, 1):
+        for copy in spread(pieces_mine.at[p], pieces_in.at[p], piece_send.at[0], piece_recv, 1, 0):
             copy.start()
+        across(pieces_mine.at[p], pieces_in.at[p], piece_send.at[0], piece_recv).start()
 
     total = functools.reduce(jnp.add, squares)
     coarse = total.astype(BF16)
@@ -693,96 +732,117 @@
     scale = lax.rsqrt(mean + EPSILON)
     scales_mine[0] = scale
     scales_mine[1] = pltpu.roll(scale, half, 1)
-    for copy in spread(scales_mine, scales_in, piece_send.at[1], piece_recv.at[2], 1):
-        copy.start()
+    for r in range(2):
+        remote(
+            scales_mine.at[r],
+            scales_in.at[2 + t],
+            piece_send.at[1],
+            scale_recv.at[1],
+            {"fs": f ^ 1, "tp": r},
+        ).start()
+    across(scales_mine, scales_in, piece_send.at[1], scale_recv).start()
+    for p in range(pairs):
+        for copy in spread(pieces_mine.at[p], pieces_in.at[p], piece_send.at[0], piece_recv, 1, 1):
+            copy.start()
+
+    far_kv(me == 0)
 
     acts_in[t] = acts_mine[t]
     for p in range(pairs):
         pieces_in[p, t] = pieces_mine[p, t]
     scales_in[t] = scales_mine[t]
 
-    for i, ref in enumerate((wat_x, wst_y)):
-        arrived(ref.at[t], weight_recv.at[i])
-        weight_copies(2)[i].start()
-
-    def groups(own, other):
-        return [(ref, slice(h * part, (h + 1) * part)) for ref in (own, other) for h in range(2)]
-
-    def back(out, landing, g, send, recv, hop):
-        return remote(out.at[g], landing.at[g], send, recv, {"fs": f ^ hop})
-
-    arrived(acts_in.at[0:3], act_sem.at[1])
-    arrived(wat, weight_recv.at[2])
-    left = jnp.concatenate(
-        [jnp.concatenate([acts_in[s], acts_in[2 + s]], axis=0) for s in range(2)], axis=1
-    )
-    for pair in (0, 2):
-        for g, (weights, at) in list(enumerate(groups(wat, wat_x)))[pair : pair + 2]:
-            right = jnp.concatenate([weights[s, :, at] for s in range(2)], axis=0)
-            product = jnp.dot(left, right, preferred_element_type=F32)
-            acc[g] = product[0:half]
-            att_out[g] = product[half:].astype(BF16)
-        for g in (pair, pair + 1):
-            back(att_out, att_in, g, sum_send.at[0], sum_recv.at[0], 2).start()
-
-    arrived(wst, weight_recv.at[3])
-    arrived(pieces_in.at[0 : pairs - 1, 0:3], piece_recv.at[0])
-    cut = (pairs - 1) * LANES
-    for s in range(2):
-        left = jnp.concatenate(
-            [
-                jnp.concatenate([pieces_in[p, s], pieces_in[p, 2 + s]], axis=0)
-                for p in range(pairs - 1)
-            ],
-            axis=1,
-        )
-        for g, (weights, at) in enumerate(groups(wst, wst_y)):
-            acc_state[g, s] = jnp.dot(left, weights[s, 0:cut, at], preferred_element_type=F32)
-
-    arrived(pieces_in.at[pairs - 1, 0:3], piece_recv.at[1])
-    arrived(scales_in.at[0:3], piece_recv.at[2])
-    upright = scales_in[...].reshape(4 * 8, rows).T
-    by = [upright[0:half, 8 * i : 8 * i + 1] for i in range(4)]
-
-    def state_sum(g, weights, at, slot):
-        here = slice(slot // 2 * half, (slot // 2 + 1) * half)
-        return functools.reduce(
-            jnp.add,
-            [
-                (
-                    acc_state[g, s, here]
-                    + jnp.dot(
-                        pieces_in[pairs - 1, slot + s],
-                        weights[s, cut:, at],
-                        preferred_element_type=F32,
-                    )
-                )
-                * by[slot + s]
-                for s in range(2)
-            ],
-        )
-
-    for pair in (0, 2):
-        for g, (weights, at) in list(enumerate(groups(wst, wst_y)))[pair : pair + 2]:
-            sum_out[g] = state_sum(g, weights, at, 2).astype(BF16)
-        for g in (pair, pair + 1):
-            back(sum_out, sum_in, g, sum_send.at[1], sum_recv.at[1], 1).start()
-
     def place(owner, h, values):
         at = pl.ds(pl.multiple_of(owner * cols + h * part, part), part)
         out_ref[0, :, at] = values.astype(BF16)
 
+    def halves(weights):
+        return [(weights, slice(h * part, (h + 1) * part)) for h in range(2)]
+
+    def attended(slot, span, weights, at):
+        left = jnp.concatenate([acts_in[slot + s, span] for s in range(2)], axis=1)
+        right = jnp.concatenate([weights[s, :, at] for s in range(2)], axis=0)
+        return jnp.dot(left, right, preferred_element_type=F32)
+
+    def mixed(slot, span, by, weights, at):
+        sums = []
+        for s in range(2):
+            left = jnp.concatenate([pieces_in[p, slot + s, span] for p in range(pairs)], axis=1)
+            sums.append(jnp.dot(left, weights[s, :, at], preferred_element_type=F32) * by[s])
+        return sums[0] + sums[1]
+
+    whole = slice(0, half)
+    arrived(wst, peer_recv.at[0])
+    arrived(acts_in.at[0], act_recv.at[0])
+    arrived(pieces_in.at[:, 0], piece_recv.at[0])
+    arrived(scales_in.at[0], scale_recv.at[0])
+    upright = scales_in[0:2].reshape(2 * 8, rows).T
+    mine = [upright[0:half, 8 * s : 8 * s + 1] for s in range(2)]
+    for h in range(2):
+        place(
+            f,
+            h,
+            attended(0, whole, *halves(wat)[h]) + mixed(0, whole, mine, *halves(wst)[h]),
+        )
+
+    for chunk in range(2):
+        for i, ref in enumerate((wat_x, wst_y)):
+            arrived(ref.at[t, chunks[chunk]], weight_recv.at[i, chunk])
+            relay_copies(chunk)[i].start()
+    arrived(wst, peer_recv.at[1])
+    for h in range(2):
+        acc[h] = attended(0, whole, *halves(wat_x)[h])
+        acc[2 + h] = mixed(0, whole, mine, *halves(wst_y)[h])
+
+    def attended_back(q):
+        return remote(
+            att_out.at[q], att_in.at[q], sum_send.at[0], sum_recv.at[0], {"fs": f ^ 2}
+        )
+
+    def mixed_back(q):
+        return remote(
+            sum_out.at[q], sum_in.at[q], sum_send.at[1], sum_recv.at[1], {"fs": f ^ 1}
+        )
+
+    def attended_step(q):
+        arrived(acts_in.at[2:4, spans[q]], act_recv.at[1 + q])
+        for g, (weights, at) in enumerate(halves(wat) + halves(wat_x)):
+            att_out[q, g] = attended(2, spans[q], weights, at).astype(BF16)
+        attended_back(q).start()
+
+    def mixed_step(q):
+        arrived(pieces_in.at[:, 2:4, spans[q]], piece_recv.at[1 + q])
+        if q == 0:
+            arrived(scales_in.at[2:4], scale_recv.at[1])
+        upright = scales_in[2:4].reshape(2 * 8, rows).T
+        by = [upright[spans[q], 8 * s : 8 * s + 1] for s in range(2)]
+        for g, (weights, at) in enumerate(halves(wst) + halves(wst_y)):
+            sum_out[q, g] = mixed(2, spans[q], by, weights, at).astype(BF16)
+        mixed_back(q).start()
+
+    @pl.when(me < sp - 1)
+    def _():
+        for q in range(2):
+            mixed_step(q)
+            attended_step(q)
+
+    @pl.when(me == sp - 1)
+    def _():
+        for q in range(2):
+            attended_step(q)
+        for q in range(2):
+            mixed_step(q)
+
+    def joined(ref, g):
+        return jnp.concatenate([ref[q, g] for q in range(2)], axis=0).astype(F32)
+
     arrived(att_in, sum_recv.at[0])
-    for g, (weights, at) in enumerate(groups(wst, wst_y)):
-        mine = state_sum(g, weights, at, 0)
-        if g < 2:
-            place(f, g, acc[g] + mine)
-        else:
-            place(f ^ 2, g - 2, att_in[g - 2].astype(F32) + mine)
+    for h in range(2):
+        place(f ^ 2, h, acc[2 + h] + joined(att_in, h))
     arrived(sum_in, sum_recv.at[1])
     for h in range(2):
-        place(f ^ 1, h, acc[2 + h] + sum_in[h].astype(F32))
-        place(f ^ 3, h, att_in[2 + h].astype(F32) + sum_in[2 + h].astype(F32))
+        place(f ^ 1, h, acc[h] + joined(sum_in, h))
+        place(f ^ 3, h, joined(att_in, 2 + h) + joined(sum_in, 2 + h))
 
     @pl.when(follows)
     def _():
@@ -798,7 +858,7 @@
 
     for kind in range(3):
         departed(wst, weight_send.at[kind])
-    departed(acts_in.at[0:3], act_sem.at[0])
+    departed(acts_in.at[0:3], act_send)
     departed(pieces_in.at[:, 0:3], piece_send.at[0])
     departed(scales_in.at[0:3], piece_send.at[1])
     departed(att_out, sum_send.at[0])
@@ -835,6 +895,7 @@
             pltpu.VMEM((8 + rows, width + 2 * STATE), F32),
             pltpu.VMEM((16, width + 2 * STATE), BF16),
             pltpu.VMEM((rows, width + 2 * STATE), BF16),
+            pltpu.VMEM((2, heads, rows), F32),
             pltpu.VMEM((rows, width), F32),
             pltpu.VMEM((sp, rows, 2 * kv_width), BF16),
             pltpu.VMEM((sp, heads, rows), F32),
@@ -854,20 +915,22 @@
             pltpu.VMEM((2, 8, rows), F32),
             pltpu.VMEM((4, 8, rows), F32),
             pltpu.VMEM((4, half, part), F32),
-            pltpu.VMEM((4, 2, rows, part), F32),
-            pltpu.VMEM((4, half, part), BF16),
-            pltpu.VMEM((4, half, part), BF16),
-            pltpu.VMEM((4, half, part), BF16),
-            pltpu.VMEM((4, half, part), BF16),
+            pltpu.VMEM((2, 4, half // 2, part), BF16),
+            pltpu.VMEM((2, 4, half // 2, part), BF16),
+            pltpu.VMEM((2, 4, half // 2, part), BF16),
+            pltpu.VMEM((2, 4, half // 2, part), BF16),
             dma((2,)),
             dma((4,)),
             dma,
             dma((pairs,)),
             dma((3,)),
-            dma((4,)),
+            dma((2, 2)),
             dma((2,)),
+            dma,
+            dma((3,)),
             dma((2,)),
             dma((3,)),
+            dma((2,)),
             dma((2,)),
             dma((2,)),
         ],

time: 26.6 us -> 27.8 us (1.045); the launches traced: 26 us -> 27.7 us
  Pallas kernels: 25.3 us -> 26.9 us
    pallas_call x1, Pallas kernels: 25.3 us -> 26.9 us  [fused(): pl.pallas_call(functools.partial(mixer_kernel, sp, fs), out_shape=pltpu.V...]
where the time goes in v4:
time: 27.8 us; the launch traced here: 27.7 us
  Pallas kernels  26.9 us (97%)
  local copies, waits for them, and re-layouts  0.71 us (3%)
    pallas_call x1, Pallas kernels, fused(): pl.pallas_call(functools.partial(mixer_kernel, sp, fs), out_shape=pltpu.V...  26.9 us
    unnamed x1, local copies, waits for them, and re-layouts  0.71 us

profile of v4, /device:TPU:24, one launch (start us, length us, event | category | flops | bytes accessed | tf_op | source)
XLA Modules:
  0.0 27.7 jit_solution(16975011912914978038)
XLA Ops:
  0.0 26.9 %shard_map.172 = bf16[1,64,2048]{2,1,0:T(8,128)(2,1)S(1)} custom-call(bf16[1,128,512]{2,1,0:T(8,128)(2,1)} %x_far.1, bf16[1,128,128]{2,1,0:T(8,128)(2,1)} %w_far.1, bf16[1,128,128]{2,1,0:T(8,128)(2,1)} %r_far.1, bf16[1,128,512]{2,1,0:T(8,128)(2,1)} %gate_far.1, f32[1,8,128]{2,1,0:T(8,128)} %step_far.1, f32[1,8,128]{2,1,0:T(8,128)} %extra_far.1, ...), custom_call_target="tpu_custom_call" | custom-call | tf_op jit(solution)/shard_map/pallas_call | solution.py:886
  27.0 0.7 %copy.20 = bf16[1,64,2048]{2,1,0:T(8,128)(2,1)} copy(bf16[1,64,2048]{2,1,0:T(8,128)(2,1)S(1)} %shard_map.172) | data formatting | bytes 524288

commit v5 on v4

--- a/solution.py
+++ b/solution.py
@@ -310,7 +310,8 @@
     sum_out,
     sum_in,
     tail_sem,
-    kv_sem,
+    kv_send,
+    kv_recv,
     st_send,
     st_recv,
     weight_send,
@@ -376,9 +377,13 @@
         "gain": (gain_far, gain_ref),
         "bypass": (bypass_far, bypass_ref),
     }
+    shared = {"v": "k", "wst": "wat"}
+    places = [name for name in near if name not in shared]
     loads = {
-        name: pltpu.make_async_copy(far, here, load_sem.at[i])
-        for i, (name, (far, here)) in enumerate(near.items())
+        name: pltpu.make_async_copy(
+            far, here, load_sem.at[places.index(shared.get(name, name))]
+        )
+        for name, (far, here) in near.items()
     }
     for load in loads.values():
         load.start()
@@ -475,15 +480,24 @@
             )
 
     deep = wst_far.shape[0]
-    chunks = (slice(0, deep * 3 // 4), slice(deep * 3 // 4, deep))
+    lent = deep * 3 // 16 // 16 * 16
+    ends = (0, lent, 2 * lent, deep * 7 // 8, deep)
+    chunks = [slice(ends[c], ends[c + 1]) for c in range(4)]
+    odd = lax.rem(me, 2) == 1
+    even = jnp.logical_not(odd)
+    top = me == sp - 1
 
     def weight_copies(chunk):
         at = (t, chunks[chunk])
         return [
             remote(
-                src.at[at], dst.at[at], weight_send.at[0], weight_recv.at[i, chunk], {"fs": f ^ hop}
-            )
-            for i, (src, dst, hop) in enumerate(((wat, wat_x, 1), (wst, wst_y, 2)))
+                src.at[at],
+                dst.at[at],
+                weight_send.at[0],
+                weight_recv.at[chunk],
+                {"fs": f ^ hop},
+            )
+            for src, dst, hop in ((wat, wat_x, 1), (wst, wst_y, 2))
         ]
 
     def own_copies():
@@ -491,15 +505,43 @@
             remote(w.at[t], w.at[t], weight_send.at[1], peer_recv.at[0], peer) for w in (wat, wst)
         ]
 
-    def relay_copies(chunk):
+    def landed(chunk):
+        arrived(wat_x.at[:, chunks[chunk]], weight_recv.at[chunk])
+
+    def relay(chunk):
+        for w in (wat_x, wst_y):
+            at = (t, chunks[chunk])
+            remote(w.at[at], w.at[at], weight_send.at[2], peer_recv.at[1], peer).start()
+
+    def lend(chunk):
         at = (t, chunks[chunk])
         return [
-            remote(w.at[at], w.at[at], weight_send.at[2], peer_recv.at[1], peer)
+            remote(
+                w.at[at],
+                w.at[at],
+                weight_send.at[3],
+                weight_recv.at[chunk],
+                {"sp": lax.rem(me + sp - 1, sp)},
+            )
             for w in (wat_x, wst_y)
         ]
 
-    loaded("wat", "wst")
-    for copy in weight_copies(0) + weight_copies(1) + own_copies():
+    pltpu.make_async_copy(wst, wst, load_sem.at[places.index("wat")]).wait()
+    for chunk, fits in (
+        (0, odd),
+        (1, even),
+        (0, jnp.logical_and(even, top)),
+        (1, jnp.logical_and(odd, top)),
+        (2, me >= 0),
+        (3, me >= 0),
+    ):
+
+        @pl.when(fits)
+        def _(chunk=chunk):
+            for copy in weight_copies(chunk):
+                copy.start()
+
+    for copy in own_copies():
         copy.start()
 
     @pl.when(me > 0)
@@ -513,13 +555,14 @@
         there = {"sp": lax.rem(me + 1, sp)}
         return remote(state_out.at[p], state_in.at[p], st_send, st_recv.at[p], there)
 
-    loaded("k", "v", "forget")
+    pltpu.make_async_copy(kvall.at[me], kvall.at[me], load_sem.at[places.index("k")]).wait()
+    loaded("forget")
     gall[me] = forget_ref[0]
     gate_cols = forget_ref[0].T
 
     tail = [
         remote(
-            ref.at[0, rows - 16 : rows, :],
+            ref.at[0, rows - 8 : rows, :],
             tails.at[:, at],
             tail_sem.at[0],
             tail_sem.at[1],
@@ -528,11 +571,11 @@
         for ref, _, at in inputs
     ]
 
-    def kv_copies(d):
+    def kv_copies(d, source, kind):
         there = {"sp": lax.rem(me + d, sp)}
         return [
-            remote(kvall.at[me], kvall.at[me], kv_sem.at[0], kv_sem.at[1], there),
-            remote(gall.at[me], gall.at[me], kv_sem.at[2], kv_sem.at[3], there),
+            remote(kvall.at[source], kvall.at[source], kv_send.at[0], kv_recv.at[kind, 0], there),
+            remote(gall.at[source], gall.at[source], kv_send.at[1], kv_recv.at[kind, 1], there),
         ]
 
     @pl.when(follows)
@@ -547,7 +590,7 @@
 
     @pl.when(follows)
     def _():
-        for copy in kv_copies(1):
+        for copy in kv_copies(1, me, 0):
             copy.start()
 
     def far_kv(fits):
@@ -556,8 +599,11 @@
             @pl.when(jnp.logical_and(fits, me + d < sp))
             def _(d=d):
                 pl.semaphore_wait(ready.at[d - 2], 1)
-                for copy in kv_copies(d):
-                    copy.start()
+
+                @pl.when(jnp.logical_or(me == 0, d > 2))
+                def _():
+                    for copy in kv_copies(d, me, 1):
+                        copy.start()
 
     far_kv(me > 0)
 
@@ -604,7 +650,7 @@
     @pl.when(me > 0)
     def _():
         arrived(tails, tail_sem.at[1])
-        pad_ref[0:8, :] = tails[...].astype(F32)[8:16]
+        pad_ref[0:8, :] = tails[...].astype(F32)
         filtered(16)
         own_states()
 
@@ -612,8 +658,8 @@
     def _():
         within()
 
-    def relay():
-        for p in range(pairs):
+    def pass_state(which):
+        for p in which:
             state_copy(p).wait_recv()
             decay = jnp.where(low, decays[2 * p : 2 * p + 1, :], decays[2 * p + 1 : 2 * p + 2, :])
             state_out[p] = (state_in[p].astype(F32) * decay + own_state[p]).astype(BF16)
@@ -621,23 +667,134 @@
 
     @pl.when(jnp.logical_and(me == 1, follows))
     def _():
-        relay()
+        pass_state(range(pairs))
 
     @pl.when(me == 1)
     def _():
         within()
 
-    for j in range(1, sp):
+    for chunk, parity in ((0, odd), (1, even)):
+
+        @pl.when(jnp.logical_and(parity, me > 0))
+        def _(chunk=chunk):
+            landed(chunk)
+            for copy in lend(chunk):
+                copy.start()
+            relay(chunk)
+
+    @pl.when(me > 0)
+    def _():
+        arrived(kvall.at[0], kv_recv.at[0, 0])
+        arrived(gall.at[0], kv_recv.at[0, 1])
+
+    @pl.when(jnp.logical_and(me > 1, follows))
+    def _():
+        for copy in kv_copies(1, me - 1, 1):
+            copy.start()
+
+    quarter = half // 2
+    spans = (slice(0, quarter), slice(quarter, half))
+
+    def spread(src, dst, send, recv, hop, q):
+        return [
+            remote(
+                src.at[r, spans[q]],
+                dst.at[2 + t, spans[q]],
+                send,
+                recv.at[1 + q],
+                {"fs": f ^ hop, "tp": r},
+            )
+            for r in range(2)
+        ]
+
+    def across(src, dst, send, recv):
+        return remote(src.at[1 - t], dst.at[t], send, recv.at[0], peer)
+
+    def second_quarter(p):
+        for copy in spread(pieces_mine.at[p], pieces_in.at[p], piece_send.at[0], piece_recv, 1, 1):
+            copy.start()
+
+    def state_part():
+        conv_read = conv[:, width + STATE :]
+        squares = []
+        for p in range(pairs):
+            at = slice(p * LANES, (p + 1) * LANES)
+
+            @pl.when(me == sp - 1)
+            def _(p=p):
+                state_copy(p).wait_recv()
+
+            carried = jnp.dot(conv_read, state_in[p], preferred_element_type=F32)
+            gate = gate_ref[0, :, at].astype(F32)
+            u = (mix[:, at] + carried * expand(exp_cum, p)) * (gate * jax.nn.sigmoid(gate))
+            squares.append(u * u)
+            sent = (u * gain_ref[0:1, at]).astype(BF16)
+            for r in range(2):
+                pieces_mine[p, r] = sent[r * half : (r + 1) * half]
+            for copy in spread(pieces_mine.at[p], pieces_in.at[p], piece_send.at[0], piece_recv, 1, 0):
+                copy.start()
+            across(pieces_mine.at[p], pieces_in.at[p], piece_send.at[0], piece_recv).start()
+
+            @pl.when(top)
+            def _(p=p):
+                second_quarter(p)
+
+        total = functools.reduce(jnp.add, squares)
+        coarse = total.astype(BF16)
+        fine = (total - coarse.astype(F32)).astype(BF16)
+        mean = (
+            lax.dot_general(
+                jnp.ones((8, 2 * LANES), BF16),
+                jnp.concatenate([coarse, fine], axis=1),
+                (((1,), (1,)), ((), ())),
+                preferred_element_type=F32,
+            )
+            / width
+        )
+        scale = lax.rsqrt(mean + EPSILON)
+        scales_mine[0] = scale
+        scales_mine[1] = pltpu.roll(scale, half, 1)
+        for r in range(2):
+            remote(
+                scales_mine.at[r],
+                scales_in.at[2 + t],
+                piece_send.at[1],
+                scale_recv.at[1],
+                {"fs": f ^ 1, "tp": r},
+            ).start()
+        across(scales_mine, scales_in, piece_send.at[1], scale_recv).start()
+
+        @pl.when(jnp.logical_not(top))
+        def _():
+            for p in range(pairs):
+                second_quarter(p)
+
+    middle = jnp.logical_and(me > 1, follows)
+    ahead = jnp.logical_and(middle, t == 1)
+    amid = jnp.logical_and(middle, t == 0)
+
+    @pl.when(ahead)
+    def _():
+        pass_state(range(pairs))
+        state_part()
+
+    for j in range(2, sp):
 
         @pl.when(me == j)
         def _(j=j):
-            arrived(kvall.at[0:j], kv_sem.at[1])
-            arrived(gall.at[0:j], kv_sem.at[3])
+            arrived(kvall.at[0 : j - 1], kv_recv.at[1, 0])
+            arrived(gall.at[0 : j - 1], kv_recv.at[1, 1])
 
     keys = kvall[:, :, 0:kv_width].reshape(sp * rows, -1)
     values = kvall[:, :, kv_width:].reshape(sp * rows, -1)
     visible = [j * rows + col_id <= me * rows + row_id for j in range(sp)]
     for kv in range(kv_heads):
+        if kv == 1:
+
+            @pl.when(amid)
+            def _():
+                pass_state(range(pairs // 2))
+
         own = lane // HEAD_DIM == kv
         summed_values = jnp.where(own, values, jnp.ones_like(values))
         scores = lax.dot_general(
@@ -656,11 +813,11 @@
                 )
                 for j in range(sp)
             ]
-            top = tiles[0]
+            peak = tiles[0]
             for tile in tiles[1:]:
-                top = jnp.maximum(top, tile)
-            top = jnp.max(top, axis=1, keepdims=True)
-            probs = jnp.concatenate([jnp.exp(tile - top).astype(BF16) for tile in tiles], axis=1)
+                peak = jnp.maximum(peak, tile)
+            peak = jnp.max(peak, axis=1, keepdims=True)
+            probs = jnp.concatenate([jnp.exp(tile - peak).astype(BF16) for tile in tiles], axis=1)
             both = jnp.dot(probs, summed_values, preferred_element_type=F32)
             turned = pltpu.roll(both, HEAD_DIM, 1)
             outs.append(both / turned if h % 2 == kv else turned / both)
@@ -670,82 +827,34 @@
             for r in range(2):
                 acts_mine[r, :, at] = merged[r * half : (r + 1) * half]
 
-    quarter = half // 2
-    spans = (slice(0, quarter), slice(quarter, half))
-
-    def spread(src, dst, send, recv, hop, q):
-        return [
-            remote(
-                src.at[r, spans[q]],
-                dst.at[2 + t, spans[q]],
-                send,
-                recv.at[1 + q],
-                {"fs": f ^ hop, "tp": r},
-            )
-            for r in range(2)
-        ]
-
-    def across(src, dst, send, recv):
-        return remote(src.at[1 - t], dst.at[t], send, recv.at[0], peer)
+    @pl.when(amid)
+    def _():
+        pass_state(range(pairs // 2, pairs))
 
     for q in range(2):
         for copy in spread(acts_mine, acts_in, act_send, act_recv, 2, q):
             copy.start()
     across(acts_mine, acts_in, act_send, act_recv).start()
 
-    @pl.when(jnp.logical_and(me > 1, follows))
-    def _():
-        relay()
-
-    conv_read = conv[:, width + STATE :]
-    squares = []
-    for p in range(pairs):
-        at = slice(p * LANES, (p + 1) * LANES)
-
-        @pl.when(me == sp - 1)
-        def _(p=p):
-            state_copy(p).wait_recv()
-
-        carried = jnp.dot(conv_read, state_in[p], preferred_element_type=F32)
-        gate = gate_ref[0, :, at].astype(F32)
-        u = (mix[:, at] + carried * expand(exp_cum, p)) * (gate * jax.nn.sigmoid(gate))
-        squares.append(u * u)
-        sent = (u * gain_ref[0:1, at]).astype(BF16)
-        for r in range(2):
-            pieces_mine[p, r] = sent[r * half : (r + 1) * half]
-        for copy in spread(pieces_mine.at[p], pieces_in.at[p], piece_send.at[0], piece_recv, 1, 0):
-            copy.start()
-        across(pieces_mine.at[p], pieces_in.at[p], piece_send.at[0], piece_recv).start()
-
-    total = functools.reduce(jnp.add, squares)
-    coarse = total.astype(BF16)
-    fine = (total - coarse.astype(F32)).astype(BF16)
-    mean = (
-        lax.dot_general(
-            jnp.ones((8, 2 * LANES), BF16),
-            jnp.concatenate([coarse, fine], axis=1),
-            (((1,), (1,)), ((), ())),
-            preferred_element_type=F32,
-        )
-        / width
-    )
-    scale = lax.rsqrt(mean + EPSILON)
-    scales_mine[0] = scale
-    scales_mine[1] = pltpu.roll(scale, half, 1)
-    for r in range(2):
-        remote(
-            scales_mine.at[r],
-            scales_in.at[2 + t],
-            piece_send.at[1],
-            scale_recv.at[1],
-            {"fs": f ^ 1, "tp": r},
-        ).start()
-    across(scales_mine, scales_in, piece_send.at[1], scale_recv).start()
-    for p in range(pairs):
-        for copy in spread(pieces_mine.at[p], pieces_in.at[p], piece_send.at[0], piece_recv, 1, 1):
-            copy.start()
-
-    far_kv(me == 0)
+    def relay_middle():
+        for chunk, parity in ((1, odd), (0, even)):
+
+            @pl.when(jnp.logical_and(parity, top))
+            def _(chunk=chunk):
+                landed(chunk)
+                relay(chunk)
+
+        @pl.when(me == 0)
+        def _():
+            landed(1)
+            relay(1)
+
+        landed(2)
+        relay(2)
+
+    @pl.when(jnp.logical_not(ahead))
+    def _():
+        state_part()
 
     acts_in[t] = acts_mine[t]
     for p in range(pairs):
@@ -759,79 +868,137 @@
     def halves(weights):
         return [(weights, slice(h * part, (h + 1) * part)) for h in range(2)]
 
-    def attended(slot, span, weights, at):
-        left = jnp.concatenate([acts_in[slot + s, span] for s in range(2)], axis=1)
+    def attended(blocks, weights, at):
+        left = jnp.concatenate(
+            [
+                jnp.concatenate([acts_in[slot + s, span] for slot, span in blocks], axis=0)
+                for s in range(2)
+            ],
+            axis=1,
+        )
         right = jnp.concatenate([weights[s, :, at] for s in range(2)], axis=0)
         return jnp.dot(left, right, preferred_element_type=F32)
 
-    def mixed(slot, span, by, weights, at):
+    def mixed(blocks, by, weights, at):
         sums = []
         for s in range(2):
-            left = jnp.concatenate([pieces_in[p, slot + s, span] for p in range(pairs)], axis=1)
-            sums.append(jnp.dot(left, weights[s, :, at], preferred_element_type=F32) * by[s])
+            left = jnp.concatenate(
+                [
+                    jnp.concatenate([pieces_in[p, slot + s, span] for slot, span in blocks], axis=0)
+                    for p in range(pairs)
+                ],
+                axis=1,
+            )
+            scale = jnp.concatenate([b[s] for b in by], axis=0)
+            sums.append(jnp.dot(left, weights[s, :, at], preferred_element_type=F32) * scale)
         return sums[0] + sums[1]
 
     whole = slice(0, half)
+
+    def own_product():
+        by = columns_of(0)
+        for h in range(2):
+            attention = attended(((0, whole),), *halves(wat)[h])
+            place(f, h, attention + mixed(((0, whole),), (by,), *halves(wst)[h]))
+
+    def columns_of(slot):
+        upright = scales_in[slot : slot + 2].reshape(2 * 8, rows).T
+        return [upright[0:half, 8 * s : 8 * s + 1] for s in range(2)]
+
     arrived(wst, peer_recv.at[0])
-    arrived(acts_in.at[0], act_recv.at[0])
-    arrived(pieces_in.at[:, 0], piece_recv.at[0])
-    arrived(scales_in.at[0], scale_recv.at[0])
-    upright = scales_in[0:2].reshape(2 * 8, rows).T
-    mine = [upright[0:half, 8 * s : 8 * s + 1] for s in range(2)]
-    for h in range(2):
-        place(
-            f,
-            h,
-            attended(0, whole, *halves(wat)[h]) + mixed(0, whole, mine, *halves(wst)[h]),
-        )
-
-    for chunk in range(2):
-        for i, ref in enumerate((wat_x, wst_y)):
-            arrived(ref.at[t, chunks[chunk]], weight_recv.at[i, chunk])
-            relay_copies(chunk)[i].start()
-    arrived(wst, peer_recv.at[1])
-    for h in range(2):
-        acc[h] = attended(0, whole, *halves(wat_x)[h])
-        acc[2 + h] = mixed(0, whole, mine, *halves(wst_y)[h])
-
-    def attended_back(q):
-        return remote(
-            att_out.at[q], att_in.at[q], sum_send.at[0], sum_recv.at[0], {"fs": f ^ 2}
-        )
-
-    def mixed_back(q):
-        return remote(
-            sum_out.at[q], sum_in.at[q], sum_send.at[1], sum_recv.at[1], {"fs": f ^ 1}
-        )
-
-    def attended_step(q):
-        arrived(acts_in.at[2:4, spans[q]], act_recv.at[1 + q])
-        for g, (weights, at) in enumerate(halves(wat) + halves(wat_x)):
-            att_out[q, g] = attended(2, spans[q], weights, at).astype(BF16)
-        attended_back(q).start()
-
-    def mixed_step(q):
-        arrived(pieces_in.at[:, 2:4, spans[q]], piece_recv.at[1 + q])
-        if q == 0:
-            arrived(scales_in.at[2:4], scale_recv.at[1])
-        upright = scales_in[2:4].reshape(2 * 8, rows).T
-        by = [upright[spans[q], 8 * s : 8 * s + 1] for s in range(2)]
-        for g, (weights, at) in enumerate(halves(wst) + halves(wst_y)):
-            sum_out[q, g] = mixed(2, spans[q], by, weights, at).astype(BF16)
-        mixed_back(q).start()
-
-    @pl.when(me < sp - 1)
-    def _():
-        for q in range(2):
-            mixed_step(q)
-            attended_step(q)
-
-    @pl.when(me == sp - 1)
-    def _():
-        for q in range(2):
-            attended_step(q)
-        for q in range(2):
-            mixed_step(q)
+
+    @pl.when(jnp.logical_not(top))
+    def _():
+        arrived(acts_in.at[0], act_recv.at[0])
+        arrived(pieces_in.at[:, 0], piece_recv.at[0])
+        arrived(scales_in.at[0], scale_recv.at[0])
+        own_product()
+
+    far_kv(me == 0)
+    relay_middle()
+
+    landed(3)
+    relay(3)
+
+    for chunk, parity in ((0, even), (1, odd)):
+
+        @pl.when(jnp.logical_and(parity, jnp.logical_not(top)))
+        def _(chunk=chunk):
+            landed(chunk)
+            relay(chunk)
+
+    def back(out, landing, qs, picked, i, hop):
+        at = (slice(qs[0], qs[-1] + 1), slice(picked[0], picked[-1] + 1))
+        return remote(out.at[at], landing.at[at], sum_send.at[i], sum_recv.at[i], {"fs": f ^ hop})
+
+    def span_of(qs):
+        return slice(spans[qs[0]].start, spans[qs[-1]].stop)
+
+    def put(out, qs, g, product):
+        for q in qs:
+            start = (q - qs[0]) * quarter
+            out[q, g] = product[start : start + quarter].astype(BF16)
+
+    def attended_step(qs, picked):
+        if 0 in picked:
+            for q in qs:
+                arrived(acts_in.at[2:4, spans[q]], act_recv.at[1 + q])
+        there = (2, span_of(qs))
+        pairings = halves(wat) + halves(wat_x)
+        for g in picked:
+            if 0 in qs and g >= 2:
+                product = attended(((0, whole), there), *pairings[g])
+                acc[g - 2] = product[0:half]
+                product = product[half:]
+            else:
+                product = attended((there,), *pairings[g])
+            put(att_out, qs, g, product)
+        back(att_out, att_in, qs, picked, 0, 2).start()
+
+    def mixed_step(qs, picked):
+        if 0 in picked:
+            for q in qs:
+                arrived(pieces_in.at[:, 2:4, spans[q]], piece_recv.at[1 + q])
+            if 0 in qs:
+                arrived(scales_in.at[2:4], scale_recv.at[1])
+        there = (2, span_of(qs))
+        by = [column[span_of(qs)] for column in columns_of(2)]
+        pairings = halves(wst) + halves(wst_y)
+        for g in picked:
+            if 0 in qs and g >= 2:
+                product = mixed(((0, whole), there), (columns_of(0), by), *pairings[g])
+                acc[g] = product[0:half]
+                product = product[half:]
+            else:
+                product = mixed((there,), (by,), *pairings[g])
+            put(sum_out, qs, g, product)
+        back(sum_out, sum_in, qs, picked, 1, 1).start()
+
+    low_groups, high_groups = (0, 1), (2, 3)
+
+    @pl.when(jnp.logical_not(top))
+    def _():
+        mixed_step((0,), low_groups)
+        attended_step((0,), low_groups)
+        arrived(wat, peer_recv.at[1])
+        mixed_step((0,), high_groups)
+        attended_step((0,), high_groups)
+        mixed_step((1,), low_groups)
+        mixed_step((1,), high_groups)
+        attended_step((1,), low_groups)
+        attended_step((1,), high_groups)
+
+    @pl.when(top)
+    def _():
+        attended_step((0, 1), low_groups)
+        arrived(wat, peer_recv.at[1])
+        arrived(acts_in.at[0], act_recv.at[0])
+        attended_step((0, 1), high_groups)
+        mixed_step((0, 1), low_groups)
+        arrived(pieces_in.at[:, 0], piece_recv.at[0])
+        arrived(scales_in.at[0], scale_recv.at[0])
+        mixed_step((0, 1), high_groups)
+        own_product()
 
     def joined(ref, g):
         return jnp.concatenate([ref[q, g] for q in range(2)], axis=0).astype(F32)
@@ -849,15 +1016,29 @@
         departed(tails, tail_sem.at[0])
         departed(state_out, st_send)
 
-    for n in range(1, sp):
-
-        @pl.when(sp - 1 - me == n)
+    for j in range(sp - 1):
+        n = sum(1 for d in range(1, sp - j) if d != 2 or j == 0) + (j > 1)
+
+        @pl.when(me == j)
         def _(n=n):
-            departed(kvall.at[0:n], kv_sem.at[0])
-            departed(gall.at[0:n], kv_sem.at[2])
-
-    for kind in range(3):
-        departed(wst, weight_send.at[kind])
+            departed(kvall.at[0:n], kv_send.at[0])
+            departed(gall.at[0:n], kv_send.at[1])
+
+    @pl.when(top)
+    def _():
+        departed(wat, weight_send.at[0])
+
+    @pl.when(jnp.logical_not(top))
+    def _():
+        departed(wat.at[:, lent:], weight_send.at[0])
+
+    departed(wst, weight_send.at[1])
+    departed(wst, weight_send.at[2])
+
+    @pl.when(me > 0)
+    def _():
+        departed(wat.at[:, chunks[0]], weight_send.at[3])
+
     departed(acts_in.at[0:3], act_send)
     departed(pieces_in.at[:, 0:3], piece_send.at[0])
     departed(scales_in.at[0:3], piece_send.at[1])
@@ -890,10 +1071,10 @@
         out_specs=pl.BlockSpec(memory_space=pltpu.VMEM),
         scratch_shapes=near
         + [
-            dma((len(args),)),
+            dma((len(args) - 2,)),
             pltpu.SemaphoreType.REGULAR((max(sp - 2, 1),)),
             pltpu.VMEM((8 + rows, width + 2 * STATE), F32),
-            pltpu.VMEM((16, width + 2 * STATE), BF16),
+            pltpu.VMEM((8, width + 2 * STATE), BF16),
             pltpu.VMEM((rows, width + 2 * STATE), BF16),
             pltpu.VMEM((2, heads, rows), F32),
             pltpu.VMEM((rows, width), F32),
@@ -920,11 +1101,12 @@
             pltpu.VMEM((2, 4, half // 2, part), BF16),
             pltpu.VMEM((2, 4, half // 2, part), BF16),
             dma((2,)),
-            dma((4,)),
+            dma((2,)),
+            dma((2, 2)),
             dma,
             dma((pairs,)),
-            dma((3,)),
-            dma((2, 2)),
+            dma((4,)),
+            dma((4,)),
             dma((2,)),
             dma,
             dma((3,)),

time: 27.8 us -> 25.7 us (0.924)
  Pallas kernels: 26.9 us -> 24.9 us
    pallas_call x1, Pallas kernels: 26.9 us -> 24.9 us  [fused(): pl.pallas_call(functools.partial(mixer_kernel, sp, fs), out_shape=pltpu.V...]
where the time goes in v5:
time: 25.7 us; the launch traced here: 25.6 us
  Pallas kernels  24.9 us (97%)
  local copies, waits for them, and re-layouts  0.71 us (3%)
    pallas_call x1, Pallas kernels, fused(): pl.pallas_call(functools.partial(mixer_kernel, sp, fs), out_shape=pltpu.V...  24.9 us
    unnamed x1, local copies, waits for them, and re-layouts  0.71 us

profile of v5, /device:TPU:24, one launch (start us, length us, event | category | flops | bytes accessed | tf_op | source)
XLA Modules:
  0.0 25.6 jit_solution(5363887757413539369)
XLA Ops:
  0.0 24.9 %shard_map.172 = bf16[1,64,2048]{2,1,0:T(8,128)(2,1)S(1)} custom-call(bf16[1,128,512]{2,1,0:T(8,128)(2,1)} %x_far.1, bf16[1,128,128]{2,1,0:T(8,128)(2,1)} %w_far.1, bf16[1,128,128]{2,1,0:T(8,128)(2,1)} %r_far.1, bf16[1,128,512]{2,1,0:T(8,128)(2,1)} %gate_far.1, f32[1,8,128]{2,1,0:T(8,128)} %step_far.1, f32[1,8,128]{2,1,0:T(8,128)} %extra_far.1, ...), custom_call_target="tpu_custom_call" | custom-call | tf_op jit(solution)/shard_map/pallas_call | solution.py:1067
  24.9 0.7 %copy.20 = bf16[1,64,2048]{2,1,0:T(8,128)(2,1)} copy(bf16[1,64,2048]{2,1,0:T(8,128)(2,1)S(1)} %shard_map.172) | data formatting | bytes 524288

commit v6 on v5

--- a/solution.py
+++ b/solution.py
@@ -290,6 +290,8 @@
     kvall,
     gall,
     qs,
+    early,
+    peaks,
     own_state,
     state_in,
     state_out,
@@ -590,7 +592,7 @@
 
     @pl.when(follows)
     def _():
-        for copy in kv_copies(1, me, 0):
+        for copy in kv_copies(1, me, jnp.where(me == 0, 2, 0)):
             copy.start()
 
     def far_kv(fits):
@@ -602,7 +604,7 @@
 
                 @pl.when(jnp.logical_or(me == 0, d > 2))
                 def _():
-                    for copy in kv_copies(d, me, 1):
+                    for copy in kv_copies(d, me, jnp.where(me == 0, 2, 1)):
                         copy.start()
 
     far_kv(me > 0)
@@ -682,7 +684,7 @@
                 copy.start()
             relay(chunk)
 
-    @pl.when(me > 0)
+    @pl.when(me > 1)
     def _():
         arrived(kvall.at[0], kv_recv.at[0, 0])
         arrived(gall.at[0], kv_recv.at[0, 1])
@@ -691,6 +693,51 @@
     def _():
         for copy in kv_copies(1, me - 1, 1):
             copy.start()
+
+    for j in range(3, sp):
+
+        @pl.when(me == j)
+        def _(j=j):
+            arrived(kvall.at[0 : j - 2], kv_recv.at[1, 0])
+            arrived(gall.at[0 : j - 2], kv_recv.at[1, 1])
+
+    visible = [j * rows + col_id <= me * rows + row_id for j in range(sp)]
+
+    def scored(kv, blocks):
+        own = lane // HEAD_DIM == kv
+        count = (blocks[-1] + 1 - blocks[0]) * rows
+        span = slice(blocks[0], blocks[-1] + 1)
+        keys = kvall[span, :, 0:kv_width].reshape(count, -1)
+        values = kvall[span, :, kv_width:].reshape(count, -1)
+        scores = lax.dot_general(
+            qs[kv], keys, (((1,), (1,)), ((), ())), preferred_element_type=F32
+        )
+        heads_tiles = []
+        for i in range(repeat):
+            h = kv * repeat + i
+            gate_col = gate_cols[:, h : h + 1]
+            heads_tiles.append(
+                [
+                    jnp.where(
+                        visible[j],
+                        scores[i * rows : (i + 1) * rows, n * rows : (n + 1) * rows]
+                        + (gate_col - gall[j, h : h + 1, :]),
+                        NEGATIVE,
+                    )
+                    for n, j in enumerate(blocks)
+                ]
+            )
+        return heads_tiles, jnp.where(own, values, jnp.ones_like(values))
+
+    for kv in range(kv_heads):
+        heads_tiles, summed_values = scored(kv, list(range(1, sp)))
+        for i, tiles in enumerate(heads_tiles):
+            peak = jnp.max(functools.reduce(jnp.maximum, tiles), axis=1, keepdims=True)
+            probs = jnp.concatenate([jnp.exp(tile - peak).astype(BF16) for tile in tiles], axis=1)
+            early[kv * repeat + i] = jnp.dot(
+                probs, summed_values, preferred_element_type=F32
+            )
+            peaks[kv * repeat + i] = jnp.broadcast_to(peak, (rows, LANES))
 
     quarter = half // 2
     spans = (slice(0, quarter), slice(quarter, half))
@@ -778,47 +825,22 @@
         pass_state(range(pairs))
         state_part()
 
-    for j in range(2, sp):
-
-        @pl.when(me == j)
-        def _(j=j):
-            arrived(kvall.at[0 : j - 1], kv_recv.at[1, 0])
-            arrived(gall.at[0 : j - 1], kv_recv.at[1, 1])
-
-    keys = kvall[:, :, 0:kv_width].reshape(sp * rows, -1)
-    values = kvall[:, :, kv_width:].reshape(sp * rows, -1)
-    visible = [j * rows + col_id <= me * rows + row_id for j in range(sp)]
+    @pl.when(me > 0)
+    def _():
+        arrived(kvall.at[0], kv_recv.at[2, 0])
+        arrived(gall.at[0], kv_recv.at[2, 1])
+
     for kv in range(kv_heads):
-        if kv == 1:
-
-            @pl.when(amid)
-            def _():
-                pass_state(range(pairs // 2))
-
-        own = lane // HEAD_DIM == kv
-        summed_values = jnp.where(own, values, jnp.ones_like(values))
-        scores = lax.dot_general(
-            qs[kv], keys, (((1,), (1,)), ((), ())), preferred_element_type=F32
-        )
+        heads_tiles, summed_values = scored(kv, [0])
         outs = []
-        for i in range(repeat):
+        for i, (tile,) in enumerate(heads_tiles):
             h = kv * repeat + i
-            gate_col = gate_cols[:, h : h + 1]
-            tiles = [
-                jnp.where(
-                    visible[j],
-                    scores[i * rows : (i + 1) * rows, j * rows : (j + 1) * rows]
-                    + (gate_col - gall[j, h : h + 1, :]),
-                    NEGATIVE,
-                )
-                for j in range(sp)
-            ]
-            peak = tiles[0]
-            for tile in tiles[1:]:
-                peak = jnp.maximum(peak, tile)
-            peak = jnp.max(peak, axis=1, keepdims=True)
-            probs = jnp.concatenate([jnp.exp(tile - peak).astype(BF16) for tile in tiles], axis=1)
-            both = jnp.dot(probs, summed_values, preferred_element_type=F32)
+            before = peaks[h]
+            peak = jnp.maximum(before, jnp.max(tile, axis=1, keepdims=True))
+            probs = jnp.exp(tile - peak).astype(BF16)
+            both = early[h] * jnp.exp(before - peak) + jnp.dot(
+                probs, summed_values, preferred_element_type=F32
+            )
             turned = pltpu.roll(both, HEAD_DIM, 1)
             outs.append(both / turned if h % 2 == kv else turned / both)
         for i in range(0, repeat, 2):
@@ -829,7 +851,7 @@
 
     @pl.when(amid)
     def _():
-        pass_state(range(pairs // 2, pairs))
+        pass_state(range(pairs))
 
     for q in range(2):
         for copy in spread(acts_mine, acts_in, act_send, act_recv, 2, q):
@@ -1081,6 +1103,8 @@
             pltpu.VMEM((sp, rows, 2 * kv_width), BF16),
             pltpu.VMEM((sp, heads, rows), F32),
             pltpu.VMEM((kv_heads, heads // kv_heads * rows, kv_width), BF16),
+            pltpu.VMEM((heads, rows, LANES), F32),
+            pltpu.VMEM((heads, rows, LANES), F32),
             pltpu.VMEM((pairs, STATE, LANES), F32),
             pltpu.VMEM((pairs, STATE, LANES), BF16),
             pltpu.VMEM((pairs, STATE, LANES), BF16),
@@ -1102,7 +1126,7 @@
             pltpu.VMEM((2, 4, half // 2, part), BF16),
             dma((2,)),
             dma((2,)),
-            dma((2, 2)),
+            dma((3, 2)),
             dma,
             dma((pairs,)),
             dma((4,)),

time: 25.7 us -> 25 us (0.973)
  Pallas kernels: 24.9 us -> 24.2 us
    pallas_call x1, Pallas kernels: 24.9 us -> 24.2 us  [fused(): pl.pallas_call(functools.partial(mixer_kernel, sp, fs), out_shape=pltpu.V...]
where the time goes in v6:
time: 25 us; the launch traced here: 24.9 us
  Pallas kernels  24.2 us (97%)
  local copies, waits for them, and re-layouts  0.71 us (3%)
    pallas_call x1, Pallas kernels, fused(): pl.pallas_call(functools.partial(mixer_kernel, sp, fs), out_shape=pltpu.V...  24.2 us
    unnamed x1, local copies, waits for them, and re-layouts  0.71 us

profile of v6, /device:TPU:24, one launch (start us, length us, event | category | flops | bytes accessed | tf_op | source)
XLA Modules:
  0.0 24.9 jit_solution(3066049051755076964)
XLA Ops:
  0.0 24.2 %shard_map.172 = bf16[1,64,2048]{2,1,0:T(8,128)(2,1)S(1)} custom-call(bf16[1,128,512]{2,1,0:T(8,128)(2,1)} %x_far.1, bf16[1,128,128]{2,1,0:T(8,128)(2,1)} %w_far.1, bf16[1,128,128]{2,1,0:T(8,128)(2,1)} %r_far.1, bf16[1,128,512]{2,1,0:T(8,128)(2,1)} %gate_far.1, f32[1,8,128]{2,1,0:T(8,128)} %step_far.1, f32[1,8,128]{2,1,0:T(8,128)} %extra_far.1, ...), custom_call_target="tpu_custom_call" | custom-call | tf_op jit(solution)/shard_map/pallas_call | solution.py:1089
  24.2 0.7 %copy.20 = bf16[1,64,2048]{2,1,0:T(8,128)(2,1)} copy(bf16[1,64,2048]{2,1,0:T(8,128)(2,1)S(1)} %shard_map.172) | data formatting | bytes 524288
